TPU v7x, 32 devices: a whole 2x2x4 slice. The times are simulated.
32 devices in a mesh: sp: 8 (over z, y), tp: 4 (over x, core).
Axes of the slice: x: 2, y: 2, z: 4, core: 2. Of those that a mesh axis runs over, the one named last changes fastest.
Arguments:
- tokens: bfloat16 [8192, 2048], P('sp', 'tp'), may hold values from -6 to 6
- input_norm_gain: float32 [2048], replicated, may hold values from 0.1 to 1.9
- pooling_input_matrix: bfloat16 [2048, 512], P(None, 'tp'), may hold values from -0.125 to 0.125
- query_projection_matrix: bfloat16 [2048, 1024], P(None, 'tp'), may hold values from -0.125 to 0.125
- key_projection_matrix: bfloat16 [2048, 1024], P(None, 'tp'), may hold values from -0.125 to 0.125
- value_projection_matrix: bfloat16 [2048, 1024], P(None, 'tp'), may hold values from -0.125 to 0.125
- output_gate_matrix: bfloat16 [2048, 1024], P(None, 'tp'), may hold values from -0.125 to 0.125
- input_gate_matrix: bfloat16 [2048, 2, 8], replicated
- forget_gate_matrix: bfloat16 [2048, 2, 8], replicated, may hold values from -0.125 to 0.125
- forget_gate_bias: float32 [2, 8], replicated
- log_forget_scale: float32 [2, 8192], P(None, 'sp'), may hold values from 0.35 to 2.8
- extra_log_forget: float32 [2, 8192], P(None, 'sp'), may hold values from -0.7 to 0, as said below
- starting_memory: float32 [2, 8, 128, 128], P(None, 'tp'), may hold values from -3 to 3
- starting_normalizer: float32 [2, 8, 128], P(None, 'tp'), may hold values from -3 to 3
- starting_log_scale: float32 [2, 8], P(None, 'tp'), may hold values from 2 to 5
- pooling_group_map: bfloat16 [4, 128, 128], replicated, may hold values from -0.5 to 0.5
- pooling_channel_scale: float32 [512], replicated, may hold values from 0.1 to 1.9
- memory_head_gain: float32 [1024], replicated, may hold values from 0.1 to 1.9
- pooling_output_matrix: bfloat16 [512, 2048], replicated, may hold values from -0.25 to 0.25
- memory_output_matrix: bfloat16 [1024, 2048], replicated, may hold values from -0.1875 to 0.1875
Outputs:
- mixed_out: bfloat16 [8192, 2048], P(('sp', 'tp'))
Inputs may be any that keep to these rules, and one draw needn't show every extreme that they name: `extra_log_forget`: at most three nonzero entries in each direction.
All inputs are finite; a program needn't handle non-finite values.
Results may differ from a plain program's by a relative error of at most 0.0091.
Values may be sent and summed in bfloat16 or wider, within the bound.
A program may use at most 128 MiB of HBM per device.

v0:
```python
import jax
import jax.numpy as jnp
from jax import lax
from jax.sharding import PartitionSpec as P

DH = 128
BLOCK = 128


NEG_BIG = -1e30
LN_EPS = 1e-05
HEAD_EPS = 1e-06
HIGHEST = lax.Precision.HIGHEST
RIM_ROWS = 8


def extended(block, sides, width):
    for axis, dim in sides:
        count = lax.axis_size(axis)
        forward = [(i, i + 1) for i in range(count - 1)]
        backward = [(target, source) for source, target in forward]
        low = lax.ppermute(
            lax.slice_in_dim(block, block.shape[dim] - width, None, axis=dim), axis, forward
        )
        high = lax.ppermute(lax.slice_in_dim(block, 0, width, axis=dim), axis, backward)
        block = jnp.concatenate([low, block, high], axis=dim)
    return block


def block_step(carried, pieces):
    memory, normer, maxlog = carried
    q_blk, k_blk, v_blk, i_blk, f_blk = pieces
    lower_mask = jnp.tril(jnp.ones((BLOCK, BLOCK), dtype=bool))
    cumulative = jnp.cumsum(f_blk, axis=-1)
    exponent = jnp.where(
        lower_mask, cumulative[:, :, None] - cumulative[:, None, :] + i_blk[:, None, :], NEG_BIG
    )
    carried_log = cumulative + maxlog[:, None]
    row_max = jnp.maximum(carried_log, exponent.max(-1))
    fading = jnp.exp(carried_log - row_max)
    scores = jnp.einsum("htd,hsd->hts", q_blk, k_blk, precision=HIGHEST) * jnp.exp(
        exponent - row_max[:, :, None]
    )
    numerator = fading[:, :, None] * jnp.einsum(
        "hvk,htk->htv", memory, q_blk, precision=HIGHEST
    ) + jnp.einsum("hts,hsv->htv", scores, v_blk, precision=HIGHEST)
    denominator = fading * jnp.einsum("hk,htk->ht", normer, q_blk, precision=HIGHEST) + scores.sum(
        -1
    )
    summed = cumulative[:, -1]
    weight_log = summed[:, None] - cumulative + i_blk
    new_max = jnp.maximum(summed + maxlog, weight_log.max(-1))
    carry_scale = jnp.exp(summed + maxlog - new_max)
    weights = jnp.exp(weight_log - new_max[:, None])
    memory = carry_scale[:, None, None] * memory + jnp.einsum(
        "hsv,hsk->hvk", v_blk * weights[:, :, None], k_blk, precision=HIGHEST
    )
    normer = carry_scale[:, None] * normer + jnp.einsum(
        "hs,hsk->hk", weights, k_blk, precision=HIGHEST
    )
    return ((memory, normer, new_max), (numerator, denominator, row_max))


def to_blocks(source):
    return jnp.moveaxis(
        source.reshape((source.shape[0], source.shape[1] // BLOCK, BLOCK) + source.shape[2:]), 1, 0
    )


def from_blocks(source):
    return jnp.moveaxis(source, 0, 1).reshape(
        (source.shape[1], source.shape[0] * source.shape[2]) + source.shape[3:]
    )


def local_pass(query_heads, key_heads, value_heads, log_in, log_forget_gate):
    head_count = query_heads.shape[0]
    head_size = query_heads.shape[2]
    initial = (
        jnp.zeros((head_count, head_size, head_size), jnp.float32),
        jnp.zeros((head_count, head_size), jnp.float32),
        jnp.full((head_count,), NEG_BIG, jnp.float32),
    )
    finals, outputs = lax.scan(
        block_step,
        initial,
        tuple(
            (
                to_blocks(member)
                for member in (query_heads, key_heads, value_heads, log_in, log_forget_gate)
            )
        ),
    )
    numerator, denominator, row_max = (from_blocks(member) for member in outputs)
    falls = jnp.cumsum(log_forget_gate, axis=1)
    return ((falls[:, -1],) + finals, (numerator, denominator, row_max, falls))


def join_states(earlier, later):
    early_fall, early_memory, early_normer, early_max = earlier
    late_fall, late_memory, late_normer, late_max = later
    merged_max = jnp.maximum(early_max + late_fall, late_max)
    early_weight = jnp.exp(early_max + late_fall - merged_max)
    late_weight = jnp.exp(late_max - merged_max)
    return (
        late_fall,
        early_weight[..., None, None] * early_memory + late_weight[..., None, None] * late_memory,
        early_weight[..., None] * early_normer + late_weight[..., None] * late_normer,
        merged_max,
    )


def prefix_from_all(gathered, position, from_later):
    falls, memories, normers, maxima = gathered
    order = jnp.arange(falls.shape[0], dtype=jnp.int32)
    inclusive = jnp.cumsum(falls, axis=0)
    exclusive = inclusive - falls
    if from_later:
        valid = order > position
        between = exclusive - inclusive[position][None]
        total_fall = inclusive[-1] - inclusive[position]
    else:
        valid = order < position
        between = exclusive[position][None] - inclusive
        total_fall = exclusive[position]
    log_weight = jnp.where(valid[:, None], maxima + between, NEG_BIG)
    joint_max = jnp.max(log_weight, axis=0)
    weights = jnp.where(valid[:, None], jnp.exp(log_weight - joint_max[None]), 0.0)
    memory = jnp.einsum("jh,jhvk->hvk", weights, memories, precision=HIGHEST)
    normer = jnp.einsum("jh,jhk->hk", weights, normers, precision=HIGHEST)
    return (total_fall, memory, normer, joint_max)


def finish(local_terms, entering, query_heads):
    numerator, denominator, row_max, falls = local_terms
    fall_in, memory, normer, max_in = entering
    state_log = falls + max_in[:, None]
    joint_max = jnp.maximum(row_max, state_log)
    local_weight = jnp.exp(row_max - joint_max)
    state_weight = jnp.exp(state_log - joint_max)
    full_numerator = local_weight[..., None] * numerator + state_weight[..., None] * jnp.einsum(
        "hvk,htk->htv", memory, query_heads, precision=HIGHEST
    )
    full_denominator = local_weight * denominator + state_weight * jnp.einsum(
        "hk,htk->ht", normer, query_heads, precision=HIGHEST
    )
    return full_numerator / jnp.maximum(jnp.abs(full_denominator), 1.0)[..., None]


def per_device(
    tokens,
    input_norm_gain,
    pooling_input_matrix,
    query_projection_matrix,
    key_projection_matrix,
    value_projection_matrix,
    output_gate_matrix,
    input_gate_matrix,
    forget_gate_matrix,
    forget_gate_bias,
    log_forget_scale,
    extra_log_forget,
    starting_memory,
    starting_normalizer,
    starting_log_scale,
    pooling_group_map,
    pooling_channel_scale,
    memory_head_gain,
    pooling_output_matrix,
    memory_output_matrix,
):
    local_rows = tokens.shape[0]
    own_width = tokens.shape[1]
    model_width = own_width * lax.axis_size("tp")
    group_index = lax.axis_index("tp")
    seq_index = lax.axis_index("sp")
    group_dim = pooling_input_matrix.shape[1]
    head_local = query_projection_matrix.shape[1] // DH
    mem_width = head_local * DH
    main_weight = jnp.concatenate(
        [
            pooling_input_matrix,
            query_projection_matrix,
            key_projection_matrix,
            value_projection_matrix,
            output_gate_matrix,
        ],
        axis=1,
    )
    gate_in = lax.dynamic_slice_in_dim(input_gate_matrix, group_index * head_local, head_local, 2)
    gate_fg = lax.dynamic_slice_in_dim(forget_gate_matrix, group_index * head_local, head_local, 2)
    gate_weight = jnp.concatenate([gate_in, gate_fg], axis=1).reshape(model_width, 4 * head_local)
    floats = tokens.astype(jnp.float32)
    row_sum, row_square = lax.psum(
        (jnp.sum(floats, axis=1), jnp.sum(floats * floats, axis=1)), "tp"
    )
    mean_row = row_sum / model_width
    variance = row_square / model_width - mean_row * mean_row
    gain_own = lax.dynamic_slice_in_dim(input_norm_gain, group_index * own_width, own_width, 0)
    normed = (
        (floats - mean_row[:, None]) * lax.rsqrt(variance + LN_EPS)[:, None] * gain_own
    ).astype(jnp.bfloat16)
    piece = lax.all_gather(normed, "tp", axis=1, tiled=True)
    projected = jnp.dot(piece, main_weight, preferred_element_type=jnp.float32)
    gate_pre = jnp.dot(piece, gate_weight, preferred_element_type=jnp.float32)
    pool_in = projected[:, :group_dim].astype(jnp.bfloat16)
    queries = projected[:, group_dim : group_dim + mem_width].astype(jnp.bfloat16)
    key_rows = projected[:, group_dim + mem_width : group_dim + 2 * mem_width].astype(jnp.bfloat16)
    value_rows = projected[:, group_dim + 2 * mem_width : group_dim + 3 * mem_width].astype(
        jnp.bfloat16
    )
    out_gate = projected[:, group_dim + 3 * mem_width :].astype(jnp.bfloat16)
    gate_pre = gate_pre.reshape(local_rows, 2, 2, head_local)
    log_in = gate_pre[:, 0]
    bias_own = lax.dynamic_slice_in_dim(forget_gate_bias, group_index * head_local, head_local, 1)
    log_forget_gate = (
        jax.nn.log_sigmoid(gate_pre[:, 1] + bias_own[None]) * log_forget_scale.T[:, :, None]
        + extra_log_forget.T[:, :, None]
    )

    def heads_of(source, factor):
        return (
            (source.astype(jnp.float32) * factor)
            .reshape(local_rows, head_local, DH)
            .transpose(1, 0, 2)
        )

    query_heads = heads_of(queries, 1.0)
    key_heads = heads_of(key_rows, DH ** (-0.5))
    value_heads = heads_of(value_rows, 1.0)
    forward_summary, forward_local = local_pass(
        query_heads, key_heads, value_heads, log_in[:, 0].T, log_forget_gate[:, 0].T
    )
    flipped_query = query_heads[:, ::-1]
    backward_summary, backward_local = local_pass(
        flipped_query,
        key_heads[:, ::-1],
        value_heads[:, ::-1],
        log_in[:, 1].T[:, ::-1],
        log_forget_gate[:, 1].T[:, ::-1],
    )
    rimmed = extended(pool_in, (("sp", 0),), RIM_ROWS).astype(jnp.float32)
    half_span = jnp.left_shift(jnp.int32(1), group_index)
    grouped = pool_in.astype(jnp.float32)
    pooled = jnp.zeros_like(grouped)
    for offset in range(-RIM_ROWS, RIM_ROWS):
        inside = ((offset >= -half_span) & (offset < half_span)).astype(jnp.float32)
        pooled = pooled + inside * rimmed[RIM_ROWS + offset : RIM_ROWS + offset + local_rows]
    positions = seq_index * local_rows + jnp.arange(local_rows, dtype=jnp.int32)
    total_rows = local_rows * lax.axis_size("sp")
    counts = (
        jnp.minimum(positions + half_span, total_rows) - jnp.maximum(positions - half_span, 0)
    ).astype(jnp.float32)
    contrast = (pooled / counts[:, None] - grouped).astype(jnp.bfloat16)
    map_own = lax.dynamic_index_in_dim(pooling_group_map, group_index, 0, keepdims=False)
    scale_own = lax.dynamic_slice_in_dim(
        pooling_channel_scale, group_index * group_dim, group_dim, 0
    )
    pool_out = (jnp.dot(contrast, map_own, preferred_element_type=jnp.float32) * scale_own).astype(
        jnp.bfloat16
    )
    stacked = tuple(
        (
            jnp.stack([forward_part, backward_part])[None]
            for forward_part, backward_part in zip(forward_summary, backward_summary)
        )
    )
    gathered = lax.all_gather(stacked, "sp", axis=0, tiled=True)
    forward_prefix = prefix_from_all(tuple((member[:, 0] for member in gathered)), seq_index, False)
    backward_prefix = prefix_from_all(tuple((member[:, 1] for member in gathered)), seq_index, True)

    def initial_state(direction):
        return (
            jnp.zeros((head_local,), jnp.float32),
            starting_memory[direction],
            starting_normalizer[direction],
            starting_log_scale[direction],
        )

    forward = finish(forward_local, join_states(initial_state(0), forward_prefix), query_heads)
    backward = finish(backward_local, join_states(initial_state(1), backward_prefix), flipped_query)
    hidden = forward + backward[:, ::-1]
    head_mean = jnp.mean(hidden, axis=-1, keepdims=True)
    head_var = jnp.mean(jnp.square(hidden - head_mean), axis=-1, keepdims=True)
    gain_heads = lax.dynamic_slice_in_dim(
        memory_head_gain, group_index * mem_width, mem_width, 0
    ).reshape(head_local, DH)
    scaled = (hidden - head_mean) * lax.rsqrt(head_var + HEAD_EPS) * gain_heads[:, None, :]
    mem_out = (
        scaled.transpose(1, 0, 2).reshape(local_rows, mem_width)
        * jax.nn.sigmoid(out_gate.astype(jnp.float32))
    ).astype(jnp.bfloat16)
    mixed = jnp.concatenate([pool_out, mem_out], axis=1)
    owned = lax.all_to_all(mixed, "tp", split_axis=0, concat_axis=1, tiled=True)
    owner_rows = owned.shape[0]
    owned = owned.reshape(owner_rows, lax.axis_size("tp"), group_dim + mem_width)
    pool_part = owned[:, :, :group_dim].reshape(owner_rows, lax.axis_size("tp") * group_dim)
    mem_part = owned[:, :, group_dim:].reshape(owner_rows, lax.axis_size("tp") * mem_width)
    result = jnp.dot(
        pool_part, pooling_output_matrix, preferred_element_type=jnp.float32
    ) + jnp.dot(mem_part, memory_output_matrix, preferred_element_type=jnp.float32)
    return result.astype(jnp.bfloat16)


def solution(mesh):
    placed = (
        P("sp", "tp"),
        P(),
        P(None, "tp"),
        P(None, "tp"),
        P(None, "tp"),
        P(None, "tp"),
        P(None, "tp"),
        P(),
        P(),
        P(),
        P(None, "sp"),
        P(None, "sp"),
        P(None, "tp", None, None),
        P(None, "tp", None),
        P(None, "tp"),
        P(),
        P(),
        P(),
        P(),
        P(),
    )
    return jax.shard_map(
        per_device, mesh=mesh, in_specs=placed, out_specs=P(("sp", "tp"), None), check_vma=False
    )
```

profile of v0, /device:TPU:0, one launch (start us, length us, event | category | flops | bytes accessed | tf_op | source)
XLA Modules:
  0.0 378.8 jit_solution(12067535441772045476)
XLA Ops:
  6.5 1.8 convert_reduce_fusion
  9.2 8.5 %all-reduce = (f32[1024]{0:T(1024)S(1)}, f32[1024]{0:T(1024)S(1)}) all-reduce(f32[1024]{0:T(1024)S(1)} %get-tuple-element.278, f32[1024]{0:T(1024)S(1)} %get-tuple-element.277), channel_id=1, replica_groups=mesh['sp'=8,'tp'=4] {'tp'}, use_global_device_ids=true, to_apply=%region_3.0 | all-reduce | flops 2048 | bytes 16384 | tf_op jit(solution)/shard_map/psum | solution.py:194
  17.7 2.6 fusion.71
  24.4 2.0 constant_dynamic-update-slice_fusion.8
  30.8 24.4 %all-gather.9.cloned.1.call-done = bf16[1024,2048]{1,0:T(8,128)(2,1)} async-done(((bf16[1024,512]{1,0:T(8,128)(2,1)}), bf16[1024,2048]{1,0:T(8,128)(2,1)}) %all-gather.9.cloned.1.call-update) | async-done | bytes 4194320 | tf_op jit(solution)/shard_map/all_gather | solution.py:203
  55.2 8.8 %convolution_convert_fusion = bf16[1024,1152]{1,0:T(8,128)(2,1)S(1)} fusion(bf16[1024,2048]{1,0:T(8,128)(2,1)} %all-gather.9.cloned.1.call-done, bf16[2048,1152]{1,0:T(8,128)(2,1)} %constant_dynamic-update-slice_fusion.4), kind=kOutput, calls=%fused_computation.112 | convolution fusion | flops 4833017856 | bytes 11272192 | tf_op jit(solution)/shard_map/dot_general | solution.py:204
  65.8 1.5 copy_bitcast_fusion
  67.2 3.5 collective-permute-start
  73.6 5.1 %rev.22 = f32[2,1024,128]{2,1,0:T(8,128)} reverse(f32[2,1024,128]{2,1,0:T(8,128)S(1)} %fusion.84), dimensions={1} | reverse | bytes 2097152 | tf_op jit(solution)/shard_map/rev | solution.py:234
  81.5 69.7 %while.42 = (s32[]{:T(128)}, f32[2,128,128]{2,1,0:T(8,128)S(1)}, f32[2,128]{1,0:T(2,128)S(1)}, f32[2]{0:T(128)S(1)}, f32[8,2,128,128]{3,2,1,0:T(8,128)}, /*index...) while((s32[]{:T(128)}, f32[2,128,128]{2,1,0:T(8,128)S(1)}, ...), condition=%wide.region_9.10_spmd.clone, body=%wide.region_4.9_spmd.clone.sunk | while | flops 202722560 | bytes 2191650 | solution.py:84
  88.8 1.4 convolution_add_fusion.7
  97.5 1.4 convolution_add_fusion.7
  106.2 1.4 convolution_add_fusion.7
  114.9 1.4 convolution_add_fusion.7
  123.7 1.4 convolution_add_fusion.7
  132.4 1.4 convolution_add_fusion.7
  149.8 1.4 convolution_add_fusion.7
  152.6 2.3 copy.192
  155.0 5.0 %rev.20 = f32[2,1024,128]{2,1,0:T(8,128)} reverse(f32[2,1024,128]{2,1,0:T(8,128)S(1)} %bitcast.510), dimensions={1} | reverse | bytes 2097152 | tf_op jit(solution)/shard_map/rev | solution.py:238
  160.0 6.8 %rev.21 = f32[2,1024,128]{2,1,0:T(8,128)S(1)} reverse(f32[2,1024,128]{2,1,0:T(8,128)} %get-tuple-element.380), dimensions={1} | reverse | bytes 2097152 | tf_op jit(solution)/shard_map/rev | solution.py:237
  167.9 69.4 %while.43 = (s32[]{:T(128)}, f32[2,128,128]{2,1,0:T(8,128)S(1)}, f32[2,128]{1,0:T(2,128)S(1)}, f32[2]{0:T(128)S(1)}, f32[8,2,128,128]{3,2,1,0:T(8,128)}, /*index...) while((s32[]{:T(128)}, f32[2,128,128]{2,1,0:T(8,128)S(1)}, ...), condition=%wide.region_20.21_spmd.clone, body=%wide.region_15.20_spmd.clone.sunk | while | flops 202722560 | bytes 2191142 | solution.py:84
  173.2 2.0 fusion.263
  181.9 2.0 fusion.263
  190.6 2.0 fusion.263
  199.3 2.0 fusion.263
  207.9 2.0 fusion.263
  216.6 2.0 fusion.263
  225.3 2.0 fusion.263
  233.9 2.0 fusion.263
  238.1 21.8 %all-gather.5 = f32[8,2,2]{2,1,0:T(2,128)S(1)} all-gather(f32[1,2,2]{2,1,0:T(2,128)S(1)} %maximum_bitcast_fusion.1), channel_id=3, replica_groups=mesh['sp'=8,'tp'=4] {'sp'}, dimensions={0}, use_global_device_ids=true | all-gather | bytes 144 | tf_op jit(solution)/shard_map/all_gather | solution.py:268
  262.3 16.7 %all-gather.4 = f32[8,2,2]{2,1,0:T(2,128)S(1)} all-gather(f32[1,2,2]{2,1,0:T(2,128)S(1)} %maximum_bitcast_fusion), channel_id=2, replica_groups=mesh['sp'=8,'tp'=4] {'sp'}, dimensions={0}, use_global_device_ids=true | all-gather | bytes 144 | tf_op jit(solution)/shard_map/all_gather | solution.py:268
  280.1 26.5 %all-gather.3 = f32[16,2,128]{2,1,0:T(2,128)S(1)} all-gather(f32[2,2,128]{2,1,0:T(2,128)S(1)} %pad_maximum_fusion.3), channel_id=5, replica_groups=mesh['sp'=8,'tp'=4] {'sp'}, dimensions={0}, use_global_device_ids=true | all-gather | bytes 18432 | tf_op jit(solution)/shard_map/all_gather | solution.py:268
  309.6 1.6 fusion.83
  312.3 2.5 copy.97
  314.8 2.4 reshape.639
  317.2 2.6 copy.94
  319.8 2.4 reshape.636
  322.2 2.8 fusion.78
  325.0 2.8 slice_bitcast_fusion.1
  327.9 1.5 fusion.79
  329.4 2.2 fusion.77
  331.6 9.5 %rev.23 = f32[2,1024,128]{1,2,0:T(8,128)} reverse(f32[2,1024,128]{1,2,0:T(8,128)} %fusion.77), dimensions={1} | reverse | bytes 2097152 | tf_op jit(solution)/shard_map/rev | solution.py:282
  341.1 2.7 fusion.81
  343.8 2.3 fusion.172
  347.4 1.6 copy.132
  351.7 15.1 %all_to_all.16 = bf16[4,256,384]{1,2,0:T(8,128)(2,1)S(1)} all-to-all(bf16[4,256,384]{1,2,0:T(8,128)(2,1)} %copy.100), channel_id=1, replica_groups=mesh['sp'=8,'tp'=4] {'tp'}, dimensions={0} | all-to-all | bytes 1572864 | tf_op jit(solution)/shard_map/all_to_all | solution.py:294
  366.8 3.5 fusion.174
  370.3 1.7 fusion.68
  (421 shorter events, 143.9 us)
Async XLA Ops:
  6.5 363.7 %copy-start = (bf16[512,2048]{1,0:T(8,128)(2,1)S(1)}, bf16[512,2048]{1,0:T(8,128)(2,1)}, u32[]{:S(2)}) copy-start(bf16[512,2048]{1,0:T(8,128)(2,1)} %param.42) | copy-start | bytes 6291460
  6.5 48.7 %all-gather.9.cloned.1.call-start = ((), (), s32[]{:S(2)}) async-start(), calls=%async_computation.1 | async-start | bytes 5242880 | tf_op jit(solution)/shard_map/all_gather | solution.py:203
  6.5 17.0 %copy-start.15 = (f32[2,8]{1,0:T(2,128)S(1)}, f32[2,8]{1,0:T(2,128)}, u32[]{:S(2)}) copy-start(f32[2,8]{1,0:T(2,128)} %param.33) | copy-start | bytes 196
  8.3 18.1 %copy-start.6 = (bf16[2048,256]{1,0:T(8,128)(2,1)S(1)}, bf16[2048,256]{1,0:T(8,128)(2,1)}, u32[]{:S(2)}) copy-start(bf16[2048,256]{1,0:T(8,128)(2,1)} %param.27) | copy-start | bytes 3145732
  20.3 304.7 %all-gather.11.cloned.1.call-start = ((), (), s32[]{:S(2)}) async-start(), calls=%async_computation.2 | async-start | bytes 2359296 | tf_op jit(solution)/shard_map/all_gather | solution.py:268
  23.0 4.5 %copy-start.7 = (bf16[2048,256]{1,0:T(8,128)(2,1)S(1)}, bf16[2048,256]{1,0:T(8,128)(2,1)}, u32[]{:S(2)}) copy-start(bf16[2048,256]{1,0:T(8,128)(2,1)} %param.28) | copy-start | bytes 3145732
  24.4 4.2 %copy-start.8 = (bf16[2048,256]{1,0:T(8,128)(2,1)S(1)}, bf16[2048,256]{1,0:T(8,128)(2,1)}, u32[]{:S(2)}) copy-start(bf16[2048,256]{1,0:T(8,128)(2,1)} %param.29) | copy-start | bytes 3145732
  27.5 2.2 copy-start.9
  64.0 3.2 copy-start.5
  64.7 7.4 %copy-start.18 = (bf16[1024,2048]{1,0:T(8,128)(2,1)S(1)}, bf16[1024,2048]{1,0:T(8,128)(2,1)}, u32[]{:S(2)}) copy-start(bf16[1024,2048]{1,0:T(8,128)(2,1)} %all-gather.9.cloned.1.call-done) | copy-start | bytes 12582916
  65.8 7.8 %copy-start.2 = (bf16[128,2,8,128]{3,2,1,0:T(8,128)(2,1)}, bf16[128,2,8,128]{3,2,1,0:T(8,128)(2,1)S(1)}, u32[]{:S(2)}) copy-start(bf16[128,2,8,128]{3,2,1,0:T(8,128)(2,1)S(1)} %get-tuple-element.376) | copy-start | bytes 1572868
  67.2 254.9 %collective-permute-start = (bf16[8,128]{1,0:T(8,128)(2,1)}, bf16[8,128]{1,0:T(8,128)(2,1)S(1)}, u32[]{:S(2)}, u32[]{:S(2)}) collective-permute-start(bf16[8,128]{1,0:T(8,128)(2,1)} %get-tuple-element.373), channel_id=1, source_target_pairs={{0,4},{4,8},{8,12},{12,16},{16,20},{20,24},{24,28},{1,5},{5,9},{9,... | collective-permute-start | bytes 6152 | tf_op jit(solution)/shard_map/ppermute | solution.py:22
  70.7 2.7 copy-start.12
  70.7 2.7 copy-start.13
  70.7 251.4 %collective-permute-start.1 = (bf16[8,128]{1,0:T(8,128)(2,1)}, bf16[8,128]{1,0:T(8,128)(2,1)S(1)}, u32[]{:S(2)}, u32[]{:S(2)}) collective-permute-start(bf16[8,128]{1,0:T(8,128)(2,1)} %get-tuple-element.374), channel_id=1, source_target_pairs={{4,0},{8,4},{12,8},{16,12},{20,16},{24,20},{28,24},{5,1},{9,5},{13... | collective-permute-start | bytes 6152 | tf_op jit(solution)/shard_map/ppermute | solution.py:25
  78.7 1.6 copy-start.4
  167.9 141.5 %copy-start.14 = (f32[2,2,128]{2,1,0:T(2,128)S(1)}, f32[2,2,128]{2,1,0:T(2,128)}, u32[]{:S(2)}) copy-start(f32[2,2,128]{2,1,0:T(2,128)} %param.37) | copy-start | bytes 6148
  237.3 73.9 %copy-start.1 = (f32[2,1024,128]{2,1,0:T(8,128)S(1)}, f32[2,1024,128]{2,1,0:T(8,128)}, u32[]{:S(2)}) copy-start(f32[2,1024,128]{2,1,0:T(8,128)} %rev.22) | copy-start | bytes 3145732
  308.3 2.8 copy-start.16
  317.2 5.0 %slice-start = ((bf16[1024,1152]{1,0:T(8,128)(2,1)}), bf16[1024,128]{1,0:T(8,128)(2,1)S(1)}, s32[]{:S(2)}) async-start(bf16[1024,1152]{1,0:T(8,128)(2,1)} %copy-done.5), calls=%async_computation.3 | async-start | bytes 524288 | tf_op jit(solution)/shard_map/slice | solution.py:206
  317.2 5.0 %copy-start.21 = (f32[128]{0:T(128)S(1)}, f32[128]{0:T(128)}, u32[]{:S(2)}) copy-start(f32[128]{0:T(128)} %dynamic_slice.64) | copy-start | bytes 1540
  325.0 4.3 %copy-start.10 = (f32[2,1024,128]{1,2,0:T(8,128)S(1)}, f32[2,1024,128]{1,2,0:T(8,128)}, u32[]{:S(2)}) copy-start(f32[2,1024,128]{1,2,0:T(8,128)} %reshape.639) | copy-start | bytes 3145732
  325.0 4.4 %copy-start.17 = (f32[2]{0:T(128)S(1)}, f32[2]{0:T(128)}, u32[]{:S(2)}) copy-start(f32[2]{0:T(128)} %copy-done.16) | copy-start | bytes 28
  325.0 4.4 %copy-start.19 = (f32[2,2,128,128]{3,2,1,0:T(8,128)S(1)}, f32[2,2,128,128]{3,2,1,0:T(8,128)}, u32[]{:S(2)}) copy-start(f32[2,2,128,128]{3,2,1,0:T(8,128)} %param.36) | copy-start | bytes 786436
  331.6 12.2 %copy-start.3 = (bf16[128,2,8,128]{3,2,1,0:T(8,128)(2,1)S(1)}, bf16[128,2,8,128]{3,2,1,0:T(8,128)(2,1)}, u32[]{:S(2)}) copy-start(bf16[128,2,8,128]{3,2,1,0:T(8,128)(2,1)} %copy-done.2) | copy-start | bytes 1572868
  331.6 12.2 %copy-start.20 = (f32[2,2,128,128]{3,2,1,0:T(8,128)S(1)}, f32[2,2,128,128]{3,2,1,0:T(8,128)}, u32[]{:S(2)}) copy-start(f32[2,2,128,128]{3,2,1,0:T(8,128)} %param.36) | copy-start | bytes 786436
  347.4 2.9 copy-start.11
Sparse Core Ops, SparseCore 0:
  20.4 34.7 all-gather.8
  238.2 50.3 all-gather.10
where the time goes:
time: 382 us; the launch traced here: 379 us
  matrix products  149 us (39%)
  blocking collectives  88.5 us (23%)
  local copies, waits for them, and re-layouts  65.2 us (17%)
  other arithmetic  31.9 us (8%)
  waiting for transfers between devices  24.5 us (6%)
  between operations  14.1 us (4%)
  starting transfers between devices  4.82 us (1%)
    all_gather x3, blocking collectives, per_device(): gathered = lax.all_gather(stacked, 'sp', axis=0, tiled=True)  65 us
    all_gather x1, waiting for transfers between devices, per_device(): piece = lax.all_gather(normed, 'tp', axis=1, tiled=True)  24.4 us
    dot_general x16, matrix products, block_step(): jnp.einsum('hts,hsv->htv', scores, v_blk, precision=HIGHEST)  24.1 us
    dot_general x16, matrix products, block_step(): jnp.einsum('hsv,hsk->hvk', v_blk * weights[:, :, None], k_blk, precision=...  22.4 us
    dot_general x16, matrix products, block_step(): jnp.einsum('htd,hsd->hts', q_blk, k_blk, precision=HIGHEST)  21.5 us
    dot_general x16, matrix products, block_step(): jnp.einsum('hvk,htk->htv', memory, q_blk, precision=HIGHEST)  21 us
    dot_general x16, matrix products, block_step(): jnp.einsum('hk,htk->ht', normer, q_blk, precision=HIGHEST)  19.4 us
    all_to_all x1, blocking collectives, per_device(): owned = lax.all_to_all(mixed, 'tp', split_axis=0, concat_axis=1, tiled=True)  15.1 us
  transfers between devices with their start and end apart: 4, of which 1 were waited for; matrix products, arithmetic and copies ran while one was open for 52% of the time, Pallas kernels for 0%

commit v1 on v0

v1 whole, which is shorter than its diff:
```python
import functools

import jax
import jax.numpy as jnp
from jax import lax
from jax.experimental import pallas as pl
from jax.experimental.pallas import tpu as pltpu
from jax.sharding import PartitionSpec as P

DH = 128
NEG_BIG = -1e30
LN_EPS = 1e-05
HEAD_EPS = 1e-06
RIM = 16
AUG = 144
VMEM = pltpu.VMEM
MESH = pl.DeviceIdType.MESH
F32 = jnp.float32
BF16 = jnp.bfloat16


def whole_vmem(count):
    return [pl.BlockSpec(memory_space=pltpu.VMEM)] * count


def project_kernel(
    tp_size, chunks,
    tokens_ref, gain_ref, wpg_hbm, wq_hbm, wk_hbm, wv_hbm, wo_hbm,
    pool_ref, gates_ref, q_ref, k_ref, v_ref, o_ref,
    held, normed, wpg, wq, wk, wv, wo,
    load_sem, far_send, far_recv, near_send, near_recv, pass_send, pass_recv,
):
    me = lax.axis_index("tp")
    far = lax.rem(me + tp_size // 2, tp_size)
    near = me + 1 - 2 * lax.rem(me, 2)
    diagonal = lax.rem(near + tp_size // 2, tp_size)
    barrier = pltpu.get_barrier_semaphore()
    for other in (far, near):
        pl.semaphore_signal(barrier, inc=1, device_id={"tp": other}, device_id_type=MESH)
    pl.semaphore_wait(barrier, 2)
    step = tokens_ref.shape[0] // chunks
    width = tokens_ref.shape[1]

    def remote(source, slot, rows, send, recv, other):
        return pltpu.make_async_remote_copy(
            src_ref=source.at[rows], dst_ref=held.at[slot, rows], send_sem=send, recv_sem=recv,
            device_id={"tp": other}, device_id_type=MESH,
        )

    spans = [pl.ds(c * step, step) for c in range(chunks)]
    to_far = [remote(tokens_ref, 1, s, far_send.at[c], far_recv.at[c], far) for c, s in enumerate(spans)]
    to_near = [remote(tokens_ref, 0, s, near_send.at[c], near_recv.at[c], near) for c, s in enumerate(spans)]
    onward = [
        remote(held.at[1], 2, s, pass_send.at[c], pass_recv.at[c], near) for c, s in enumerate(spans)
    ]
    for c in range(chunks):
        to_far[c].start()
    loads = [
        pltpu.make_async_copy(source, target, load_sem.at[i])
        for i, (source, target) in enumerate(
            ((wpg_hbm, wpg), (wq_hbm, wq), (wk_hbm, wk), (wv_hbm, wv), (wo_hbm, wo))
        )
    ]
    for load in loads:
        load.start()
    for c in range(chunks):
        to_near[c].start()
    owners = (me, near, far, diagonal)
    model_width = width * tp_size
    for c, rows in enumerate(spans):
        to_far[c].wait_recv()
        onward[c].start()
        to_near[c].wait_recv()
        onward[c].wait_recv()
        views = [tokens_ref[rows, :]] + [held[slot, rows, :] for slot in range(3)]
        total = jnp.zeros((step, 1), F32)
        square = jnp.zeros((step, 1), F32)
        for view in views:
            part = view.astype(F32)
            total = total + jnp.sum(part, axis=1, keepdims=True)
            square = square + jnp.sum(part * part, axis=1, keepdims=True)
        mean = total / model_width
        inverse = lax.rsqrt(square / model_width - mean * mean + LN_EPS)
        for view, owner in zip(views, owners):
            columns = pl.ds(pl.multiple_of(owner * width, width), width)
            normed[:, columns] = (
                (view.astype(F32) - mean) * inverse * gain_ref[:, columns]
            ).astype(BF16)
        if c == 0:
            for load in loads:
                load.wait()
        x = normed[...]
        both = jnp.dot(x, wpg[...], preferred_element_type=F32)
        pool_ref[rows, :] = both[:, : pool_ref.shape[1]].astype(BF16)
        gates_ref[rows, :] = both[:, pool_ref.shape[1] :]
        for weight, target in ((wq, q_ref), (wk, k_ref), (wv, v_ref), (wo, o_ref)):
            target[rows, :] = jnp.dot(x, weight[...], preferred_element_type=F32).astype(BF16)
    for c in range(chunks):
        to_far[c].wait_send()
        to_near[c].wait_send()
        onward[c].wait_send()


def scan_lanes(values, combine, neutral, forward_rows):
    lanes = values.shape[1]
    lane = lax.broadcasted_iota(jnp.int32, values.shape, 1)
    forward = lax.broadcasted_iota(jnp.int32, values.shape, 0) < forward_rows
    shift = 1
    while shift < lanes:
        low = jnp.where(lane >= shift, pltpu.roll(values, shift, 1), neutral)
        high = jnp.where(lane < lanes - shift, pltpu.roll(values, lanes - shift, 1), neutral)
        values = combine(values, jnp.where(forward, low, high))
        shift *= 2
    return values


def memory_kernel(
    sp_size, heads, blocks,
    pool_ref, gates_ref, q_ref, k_ref, v_ref, o_ref, scale_ref, extra_ref, bias_ref,
    start_mem, start_norm, start_log, map_ref, pscale_ref, hgain_ref,
    out_ref,
    states, a_ref, acol_ref, locals_ref, inc_t, inc_s, exc_t, exc_s,
    send_t, send_s, recv_t, recv_s, rims, ext,
    ts, tr, ss, sr, rs, rr,
):
    me = lax.axis_index("sp")
    group = lax.axis_index("tp")
    rows_total = q_ref.shape[0]
    size = rows_total // blocks
    pairs = 2 * heads
    strides = []
    stride = 1
    while stride < sp_size:
        strides.append(stride)
        stride *= 2
    barrier = pltpu.get_barrier_semaphore()
    for stride in strides:
        for okay, other in ((me + stride < sp_size, me + stride), (me >= stride, me - stride)):
            @pl.when(okay)
            def _():
                pl.semaphore_signal(barrier, inc=1, device_id={"sp": other}, device_id_type=MESH)

    turned = jnp.transpose(gates_ref[...])
    log_in = turned[0:pairs]
    pre = turned[pairs : 2 * pairs] + bias_ref[...]
    log_sig = jnp.minimum(pre, 0.0) - jnp.log1p(jnp.exp(-jnp.abs(pre)))
    per_row = lambda ref: jnp.concatenate(
        [jnp.broadcast_to(ref[r : r + 1, :], (heads, rows_total)) for r in range(2)], axis=0
    )
    log_fg = log_sig * per_row(scale_ref) + per_row(extra_ref)
    falls = scan_lanes(log_fg, jnp.add, 0.0, heads)
    lifted = log_in - falls
    peaks = scan_lanes(lifted, jnp.maximum, NEG_BIG, heads)
    a_ref[...] = lifted + jnp.log(F32(DH ** -0.5))
    acol_ref[...] = jnp.transpose(
        jnp.concatenate([peaks, jnp.zeros((128 - pairs, rows_total), F32)], axis=0)
    )

    for h in range(heads):
        cols = slice(h * DH, (h + 1) * DH)
        vt = jnp.concatenate(
            [jnp.transpose(v_ref[:, cols].astype(F32)), jnp.ones((AUG - DH, rows_total), F32)], axis=0
        )
        for r in range(2):
            p = r * heads + h
            state = None
            before = None
            for n in range(blocks):
                b = n if r == 0 else blocks - 1 - n
                span = slice(b * size, (b + 1) * size)
                last = (b + 1) * size - 1 if r == 0 else b * size
                after = peaks[p : p + 1, last : last + 1]
                weight = jnp.exp(a_ref[p : p + 1, span] - after)
                add = jnp.dot(
                    (vt[:, span] * weight).astype(BF16), k_ref[span, cols], preferred_element_type=F32
                )
                if n > 0:
                    states[p, b] = state
                    state = jnp.exp(before - after) * state + add
                else:
                    state = add
                before = after
            end = rows_total - 1 if r == 0 else 0
            fall = falls[p : p + 1, end : end + 1]
            inc_t[p] = state
            inc_s[r, h : h + 1, :] = jnp.broadcast_to(before + fall, (1, 128))
            inc_s[r, heads + h : heads + h + 1, :] = jnp.broadcast_to(fall, (1, 128))
            exc_t[p] = jnp.zeros((AUG, DH), F32)
            exc_s[r, h : h + 1, :] = jnp.full((1, 128), NEG_BIG, F32)
            exc_s[r, heads + h : heads + h + 1, :] = jnp.zeros((1, 128), F32)

    peers = jnp.int32(0)
    for stride in strides:
        peers = peers + (me + stride < sp_size).astype(jnp.int32) + (me >= stride).astype(jnp.int32)
    pl.semaphore_wait(barrier, peers)

    def copies(level, r, other):
        t = pltpu.make_async_remote_copy(
            src_ref=send_t.at[level, r], dst_ref=recv_t.at[level, r], send_sem=ts.at[level, r],
            recv_sem=tr.at[level, r], device_id={"sp": other}, device_id_type=MESH,
        )
        s = pltpu.make_async_remote_copy(
            src_ref=send_s.at[level, r], dst_ref=recv_s.at[level, r], send_sem=ss.at[level, r],
            recv_sem=sr.at[level, r], device_id={"sp": other}, device_id_type=MESH,
        )
        return (t, s)

    def ends(level, r):
        stride = strides[level]
        if r == 0:
            return (me + stride < sp_size, me + stride, me >= stride)
        return (me >= stride, me - stride, me + stride < sp_size)

    def send(level):
        for r in range(2):
            okay, other, _unused = ends(level, r)
            send_s[level, r] = inc_s[r]
            for h in range(heads):
                send_t[level, r, h] = inc_t[r * heads + h].astype(BF16)

            @pl.when(okay)
            def _():
                for copy in copies(level, r, other):
                    copy.start()

    def fold(level, r, t_ref, s_ref):
        for h in range(heads):
            p = r * heads + h
            early_max = recv_s[level, r, h : h + 1, :]
            early_fall = recv_s[level, r, heads + h : heads + h + 1, :]
            late_max = s_ref[r, h : h + 1, :]
            late_fall = s_ref[r, heads + h : heads + h + 1, :]
            top = jnp.maximum(early_max + late_fall, late_max)
            t_ref[p] = (
                jnp.exp(early_max + late_fall - top) * recv_t[level, r, h].astype(F32)
                + jnp.exp(late_max - top) * t_ref[p]
            )
            s_ref[r, h : h + 1, :] = top
            s_ref[r, heads + h : heads + h + 1, :] = early_fall + late_fall

    def receive(level):
        for r in range(2):
            okay, other, has = ends(level, r)

            @pl.when(has)
            def _():
                for copy in copies(level, r, other):
                    copy.wait_recv()
                fold(level, r, exc_t, exc_s)
                if level + 1 < len(strides):
                    fold(level, r, inc_t, inc_s)

    def rim(side):
        rows = pl.ds(rows_total - RIM, RIM) if side == 0 else pl.ds(0, RIM)
        other = me + 1 if side == 0 else me - 1
        return pltpu.make_async_remote_copy(
            src_ref=pool_ref.at[rows], dst_ref=rims.at[side], send_sem=rs.at[side],
            recv_sem=rr.at[side], device_id={"sp": other}, device_id_type=MESH,
        )

    rim_sends = (me + 1 < sp_size, me >= 1)
    rim_recvs = (me >= 1, me + 1 < sp_size)

    def local_head(h):
        cols = slice(h * DH, (h + 1) * DH)
        t_at = lax.broadcasted_iota(jnp.int32, (size, size), 0)
        s_at = lax.broadcasted_iota(jnp.int32, (size, size), 1)
        for b in range(blocks):
            span = slice(b * size, (b + 1) * size)
            queries = q_ref[span, cols]
            scores = lax.dot_general(
                queries, k_ref[span, cols], (((1,), (1,)), ((), ())), preferred_element_type=F32
            )
            values = jnp.concatenate([v_ref[span, cols], jnp.ones((size, DH), BF16)], axis=1)
            for r in range(2):
                p = r * heads + h
                peak = acol_ref[span, p : p + 1]
                inside = (s_at <= t_at) if r == 0 else (s_at >= t_at)
                weight = jnp.exp(jnp.where(inside, a_ref[p : p + 1, span] - peak, NEG_BIG))
                part = jnp.dot((scores * weight).astype(BF16), values, preferred_element_type=F32)
                inner = b > 0 if r == 0 else b < blocks - 1
                if inner:
                    edge = b * size - 1 if r == 0 else (b + 1) * size
                    base = acol_ref[edge : edge + 1, p : p + 1]
                    part = part + jnp.exp(base - peak) * against(queries, states[p, b])
                locals_ref[p, span, :] = part

    def against(queries, state):
        spread = jnp.concatenate(
            [state[:DH], jnp.broadcast_to(state[DH : DH + 1], (DH, DH))], axis=0
        ).astype(BF16)
        return lax.dot_general(
            queries, spread, (((1,), (1,)), ((), ())), preferred_element_type=F32
        )

    def pooling():
        for side in range(2):
            @pl.when(rim_recvs[side])
            def _():
                rim(side).wait_recv()
                at = 0 if side == 0 else RIM + rows_total
                ext[at : at + RIM, :] = rims[side].astype(F32)

            @pl.when(jnp.logical_not(rim_recvs[side]))
            def _():
                at = 0 if side == 0 else RIM + rows_total
                ext[at : at + RIM, :] = jnp.zeros((RIM, ext.shape[1]), F32)
        own = pool_ref[...].astype(F32)
        ext[RIM : RIM + rows_total, :] = own
        half = jnp.left_shift(jnp.int32(1), group)
        pooled = jnp.zeros_like(own)
        reach = RIM // 2
        for offset in range(-reach, reach):
            use = jnp.logical_and(offset >= -half, offset < half).astype(F32)
            pooled = pooled + use * ext[RIM + offset : RIM + offset + rows_total, :]
        position = me * rows_total + lax.broadcasted_iota(jnp.int32, own.shape, 0)
        count = jnp.minimum(position + half, rows_total * sp_size) - jnp.maximum(position - half, 0)
        contrast = (pooled / count.astype(F32) - own).astype(BF16)
        mapped = jnp.dot(contrast, map_ref[...], preferred_element_type=F32)
        width = map_ref.shape[1]
        out_ref[:, :width] = (mapped * pscale_ref[...]).astype(BF16)

    for side in range(2):
        @pl.when(rim_sends[side])
        def _():
            rim(side).start()

    work = [functools.partial(local_head, h) for h in range(heads)] + [pooling]
    for level in range(len(strides)):
        send(level)
        if work:
            work.pop(0)()
        receive(level)
    for item in work:
        item()

    width = map_ref.shape[1]
    for h in range(heads):
        cols = slice(h * DH, (h + 1) * DH)
        enter = []
        for r in range(2):
            p = r * heads + h
            begin = start_log[p : p + 1, :]
            late_max = exc_s[r, h : h + 1, :]
            late_fall = exc_s[r, heads + h : heads + h + 1, :]
            top = jnp.maximum(begin + late_fall, late_max)
            early = jnp.exp(begin + late_fall - top)
            late = jnp.exp(late_max - top)
            mem = early * start_mem[p] + late * exc_t[p, :DH, :]
            norm = early * start_norm[p : p + 1, :] + late * exc_t[p, DH : DH + 1, :]
            enter.append(
                (jnp.concatenate([mem, jnp.broadcast_to(norm, (DH, DH))], axis=0).astype(BF16), top[:, 0:1])
            )
        for b in range(blocks):
            span = slice(b * size, (b + 1) * size)
            queries = q_ref[span, cols]
            hidden = jnp.zeros((size, DH), F32)
            for r in range(2):
                p = r * heads + h
                spread, top = enter[r]
                peak = acol_ref[span, p : p + 1]
                joint = jnp.maximum(peak, top)
                full = jnp.exp(peak - joint) * locals_ref[p, span, :] + jnp.exp(
                    top - joint
                ) * lax.dot_general(
                    queries, spread, (((1,), (1,)), ((), ())), preferred_element_type=F32
                )
                hidden = hidden + full[:, :DH] / jnp.maximum(jnp.abs(full[:, DH:]), 1.0)
            centered = hidden - jnp.mean(hidden, axis=1, keepdims=True)
            spread_sq = jnp.mean(centered * centered, axis=1, keepdims=True)
            gate = 1.0 / (1.0 + jnp.exp(-o_ref[span, cols].astype(F32)))
            out_ref[span, width + h * DH : width + (h + 1) * DH] = (
                centered * lax.rsqrt(spread_sq + HEAD_EPS) * hgain_ref[:, cols] * gate
            ).astype(BF16)

    for level in range(len(strides)):
        for r in range(2):
            okay, other, _unused = ends(level, r)

            @pl.when(okay)
            def _():
                for copy in copies(level, r, other):
                    copy.wait_send()
    for side in range(2):
        @pl.when(rim_sends[side])
        def _():
            rim(side).wait_send()


def per_device(
    tokens,
    input_norm_gain,
    pooling_input_matrix,
    query_projection_matrix,
    key_projection_matrix,
    value_projection_matrix,
    output_gate_matrix,
    input_gate_matrix,
    forget_gate_matrix,
    forget_gate_bias,
    log_forget_scale,
    extra_log_forget,
    starting_memory,
    starting_normalizer,
    starting_log_scale,
    pooling_group_map,
    pooling_channel_scale,
    memory_head_gain,
    pooling_output_matrix,
    memory_output_matrix,
):
    rows, own_width = tokens.shape
    tp_size = lax.axis_size("tp")
    sp_size = lax.axis_size("sp")
    model_width = own_width * tp_size
    group = lax.axis_index("tp")
    group_dim = pooling_input_matrix.shape[1]
    heads = query_projection_matrix.shape[1] // DH
    mem_width = heads * DH
    pairs = 2 * heads
    gate_in = lax.dynamic_slice_in_dim(input_gate_matrix, group * heads, heads, 2)
    gate_fg = lax.dynamic_slice_in_dim(forget_gate_matrix, group * heads, heads, 2)
    gate_weight = jnp.concatenate([gate_in, gate_fg], axis=1).reshape(model_width, 2 * pairs)
    wpg = jnp.concatenate(
        [pooling_input_matrix, gate_weight, jnp.zeros((model_width, 128 - 2 * pairs), BF16)], axis=1
    )
    chunks = 4
    anywhere = pl.BlockSpec(memory_space=pl.ANY)
    pool_in, gates, queries, keys, values, out_gate = pl.pallas_call(
        functools.partial(project_kernel, tp_size, chunks),
        out_shape=[
            jax.ShapeDtypeStruct((rows, group_dim), BF16),
            jax.ShapeDtypeStruct((rows, 128), F32),
        ]
        + [jax.ShapeDtypeStruct((rows, mem_width), BF16)] * 4,
        in_specs=whole_vmem(2) + [anywhere] * 5,
        out_specs=whole_vmem(6),
        scratch_shapes=[
            VMEM((3, rows, own_width), BF16),
            VMEM((rows // chunks, model_width), BF16),
            VMEM((model_width, group_dim + 128), BF16),
        ]
        + [VMEM((model_width, mem_width), BF16)] * 4
        + [pltpu.SemaphoreType.DMA((5,))]
        + [pltpu.SemaphoreType.DMA((chunks,))] * 6,
        compiler_params=pltpu.CompilerParams(
            collective_id=0, has_side_effects=True, vmem_limit_bytes=48 * 1024 * 1024
        ),
    )(
        tokens,
        input_norm_gain.reshape(1, model_width),
        wpg,
        query_projection_matrix,
        key_projection_matrix,
        value_projection_matrix,
        output_gate_matrix,
    )
    bias = lax.dynamic_slice_in_dim(forget_gate_bias, group * heads, heads, 1).reshape(pairs, 1)
    start_log = jnp.broadcast_to(starting_log_scale.reshape(pairs, 1), (pairs, 128))
    map_own = lax.dynamic_index_in_dim(pooling_group_map, group, 0, keepdims=False)
    pscale = lax.dynamic_slice_in_dim(pooling_channel_scale, group * group_dim, group_dim, 0)
    hgain = lax.dynamic_slice_in_dim(memory_head_gain, group * mem_width, mem_width, 0)
    levels = max(1, (sp_size - 1).bit_length())
    blocks = rows // 256
    mixed = pl.pallas_call(
        functools.partial(memory_kernel, sp_size, heads, blocks),
        out_shape=jax.ShapeDtypeStruct((rows, group_dim + mem_width), BF16),
        in_specs=whole_vmem(15),
        out_specs=pl.BlockSpec(memory_space=pltpu.VMEM),
        scratch_shapes=[
            VMEM((pairs, blocks, AUG, DH), F32),
            VMEM((pairs, rows), F32),
            VMEM((rows, 128), F32),
            VMEM((pairs, rows, 2 * DH), F32),
            VMEM((pairs, AUG, DH), F32),
            VMEM((2, 2 * heads, 128), F32),
            VMEM((pairs, AUG, DH), F32),
            VMEM((2, 2 * heads, 128), F32),
            VMEM((levels, 2, heads, AUG, DH), BF16),
            VMEM((levels, 2, 2 * heads, 128), F32),
            VMEM((levels, 2, heads, AUG, DH), BF16),
            VMEM((levels, 2, 2 * heads, 128), F32),
            VMEM((2, RIM, group_dim), BF16),
            VMEM((rows + 2 * RIM, group_dim), F32),
        ]
        + [pltpu.SemaphoreType.DMA((levels, 2))] * 4
        + [pltpu.SemaphoreType.DMA((2,))] * 2,
        compiler_params=pltpu.CompilerParams(
            collective_id=1, has_side_effects=True, vmem_limit_bytes=48 * 1024 * 1024
        ),
    )(
        pool_in,
        gates,
        queries,
        keys,
        values,
        out_gate,
        log_forget_scale,
        extra_log_forget,
        bias,
        starting_memory.reshape(pairs, DH, DH),
        starting_normalizer.reshape(pairs, DH),
        start_log,
        map_own,
        pscale.reshape(1, group_dim),
        hgain.reshape(1, mem_width),
    )
    owned = lax.all_to_all(mixed, "tp", split_axis=0, concat_axis=1, tiled=True)
    owner_rows = owned.shape[0]
    owned = owned.reshape(owner_rows, tp_size, group_dim + mem_width)
    pool_part = owned[:, :, :group_dim].reshape(owner_rows, tp_size * group_dim)
    mem_part = owned[:, :, group_dim:].reshape(owner_rows, tp_size * mem_width)
    result = jnp.dot(
        pool_part, pooling_output_matrix, preferred_element_type=F32
    ) + jnp.dot(mem_part, memory_output_matrix, preferred_element_type=F32)
    return result.astype(BF16)


def solution(mesh):
    placed = (
        P("sp", "tp"),
        P(),
        P(None, "tp"),
        P(None, "tp"),
        P(None, "tp"),
        P(None, "tp"),
        P(None, "tp"),
        P(),
        P(),
        P(),
        P(None, "sp"),
        P(None, "sp"),
        P(None, "tp", None, None),
        P(None, "tp", None),
        P(None, "tp"),
        P(),
        P(),
        P(),
        P(),
        P(),
    )
    return jax.shard_map(
        per_device, mesh=mesh, in_specs=placed, out_specs=P(("sp", "tp"), None), check_vma=False
    )
```

time: 382 us -> 83.4 us (0.22)
  matrix products: 149 us -> 5.17 us
  blocking collectives: 88.5 us -> 15.1 us
  local copies, waits for them, and re-layouts: 65.2 us -> 7.46 us
  Pallas kernels: 0 us -> 53.7 us
  other arithmetic: 31.9 us -> 1.48 us
  waiting for transfers between devices: 24.5 us -> 0 us
  between operations: 14.1 us -> 0.13 us
  starting transfers between devices: 4.82 us -> 0 us
    dot_general x109 -> x2, matrix products: 149 us -> 5.17 us  [the longest x1 3.46 us: per_device(): jnp.dot(mem_part, memory_output_matrix, preferred_element_type=F32)]
    all_gather x3 -> x0, blocking collectives: 65 us -> none  [per_device(): gathered = lax.all_gather(stacked, 'sp', axis=0, tiled=True)]
    pallas_call x0 -> x2, Pallas kernels: none -> 53.7 us  [the longest x1 30.5 us: per_device(): pl.pallas_call(functools.partial(project_kernel, tp_size, chunks), out_sh...]
    rev x6 -> x0, local copies, waits for them, and re-layouts: 27.8 us -> none  [the longest x1 9.46 us: per_device(): hidden = forward + backward[:, ::-1]]
    all_gather x2 -> x0, waiting for transfers between devices: 24.4 us -> none  [the longest x1 24.4 us: per_device(): piece = lax.all_gather(normed, 'tp', axis=1, tiled=True)]
    psum x1 -> x0, blocking collectives: 8.5 us -> none  [per_device(): lax.psum((jnp.sum(floats, axis=1), jnp.sum(floats * floats, axis=1)), 'tp')]
    reshape x6 -> x4, local copies, waits for them, and re-layouts: 9.73 us -> 1.86 us  [the longest x2 1.02 us: per_device(): jnp.concatenate([gate_in, gate_fg], axis=1).reshape(model_width, 2 * pairs)]
    another operation x24 -> x0, other arithmetic: 7.51 us -> none  [the longest x16 4.93 us: block_step(): cumulative = jnp.cumsum(f_blk, axis=-1)]
  transfers between devices with their start and end apart: 4 -> 0, of which waited for: 1 -> 0; matrix products, arithmetic and copies ran while one was open for 52% -> 0% of each run, Pallas kernels for 0% -> 0%
where the time goes in v1:
time: 83.4 us; the launch traced here: 83 us
  Pallas kernels  53.7 us (64%)
  blocking collectives  15.1 us (18%)
  local copies, waits for them, and re-layouts  7.46 us (9%)
  matrix products  5.17 us (6%)
  other arithmetic  1.48 us (2%)
    pallas_call x1, Pallas kernels, per_device(): pl.pallas_call(functools.partial(project_kernel, tp_size, chunks), out_sh...  30.5 us
    pallas_call x1, Pallas kernels, per_device(): pl.pallas_call(functools.partial(memory_kernel, sp_size, heads, blocks),...  23.2 us
    all_to_all x1, blocking collectives, per_device(): owned = lax.all_to_all(mixed, 'tp', split_axis=0, concat_axis=1, tiled=True)  15.1 us
    dot_general x1, matrix products, per_device(): jnp.dot(mem_part, memory_output_matrix, preferred_element_type=F32)  3.46 us
    dot_general x1, matrix products, per_device(): jnp.dot(pool_part, pooling_output_matrix, preferred_element_type=F32)  1.72 us

profile of v1, /device:TPU:0, one launch (start us, length us, event | category | flops | bytes accessed | tf_op | source)
XLA Modules:
  0.0 83.0 jit_solution(8462219825721141565)
XLA Ops:
  0.0 0.0 copy-start
  0.0 0.0 copy-start.4
  0.0 0.0 copy-start.1
  0.0 1.1 %constant_dynamic-slice_fusion.1 = (bf16[2048,2,2]{0,2,1:T(2,128)(2,1)S(1)}, bf16[2048,2,2]{0,2,1:T(2,128)(2,1)S(1)}) fusion(bf16[2048,2,8]{0,2,1:T(8,128)(2,1)} %param.28, s32[]{:T(128)S(6)} %select_n.15, bf16[2048,2,8]{0,2,1:T(8,128)(2,1)} %param.27), kind=kLoop, calls=%fused_computation.6 | loop fusion | bytes 65540 | tf_op jit(solution)/shard_map/dynamic_slice | solution.py:422
  1.1 1.0 %copy.23 = bf16[2048,8]{1,0:T(8,128)(2,1)} copy(bf16[2048,8]{0,1:T(8,128)(2,1)S(1)} %reshape.35) | data formatting | bytes 65536 | tf_op jit(solution)/shard_map/reshape | solution.py:423
  2.2 0.7 constant_dynamic-slice_fusion
  2.9 0.1 reshape.43.bias_ref
  3.0 0.8 broadcast_in_dim.11
  3.8 0.1 pad.2.clone
  3.8 0.8 dynamic_slice.24
  4.6 0.8 dynamic-slice_bitcast_fusion.1.pscale_ref
  5.3 0.0 copy-start.2
  5.3 0.8 %dynamic-slice_bitcast_fusion.map_ref = bf16[128,128]{1,0:T(8,128)(2,1)S(1)} fusion(bf16[4,128,128]{2,1,0:T(8,128)(2,1)} %param.35, s32[]{:T(128)S(6)} %select_n.16), kind=kLoop, calls=%fused_computation.4 | loop fusion | bytes 65540 | tf_op jit(solution)/shard_map/jit(dynamic_index_in_dim)/squeeze | solution.py:460
  6.2 1.4 %maximum_maximum_fusion.wpg_hbm = bf16[2048,256]{1,0:T(8,128)(2,1)S(1)} fusion(bf16[2048,8]{1,0:T(8,128)(2,1)} %copy.23, bf16[2048,128]{1,0:T(8,128)(2,1)} %param.22, bf16[256]{0:T(256)(128)(2,1)S(1)} %pad.2.clone), kind=kLoop, calls=%fused_computation.2 | loop fusion | flops 3145728 | bytes 1606144 | tf_op jit(solution)/shard_map/concatenate | solution.py:424
  7.6 0.0 copy-done.4
  7.6 0.0 copy-done.1
  7.7 0.0 copy-done.2
  7.7 0.0 copy-start.3
  7.7 0.0 copy-start.5
  7.7 0.0 copy-start.6
  7.7 0.0 copy-start.7
  7.7 30.5 %shard_map.190 = (bf16[1024,128]{1,0:T(8,128)(2,1)S(1)}, f32[1024,128]{1,0:T(8,128)S(1)}, bf16[1024,256]{1,0:T(8,128)(2,1)S(1)}, bf16[1024,256]{1,0:T(8,128)(2,1...) custom-call(bf16[1024,512]{1,0:T(8,128)(2,1)S(1)} %copy-done.1, f32[1,2048]{1,0:T(1,128)S(1)} %bitcast.20, ...), custom_call_target="tpu_custom_call" | custom-call | tf_op jit(solution)/shard_map/pallas_call | solution.py:429
  38.2 0.1 broadcast_in_dim.12.start_log
  38.3 0.0 copy-done.3
  38.3 0.0 copy-done.5
  38.3 0.0 copy-done.6
  38.3 0.0 copy-done.7
  38.3 23.2 %shard_map.191 = bf16[1024,384]{1,0:T(8,128)(2,1)S(1)} custom-call(bf16[1024,128]{1,0:T(8,128)(2,1)S(1)} %get-tuple-element.11.pool_ref, f32[1024,128]{1,0:T(8,128)S(1)} %get-tuple-element.12.gates_ref, bf16[1024,256]{1,0:T(8,128)(2,1)S(1)} %get-tuple-element.13.q_ref, bf16[1024,256]{1,0:T(8,128)(2,1)S(1)} %get-tuple-element.14.k_ref, ...), custom_call_target="tpu_custom_call" | custom-call | tf_op jit(solution)/shard_map/pallas_call | solution.py:465
  61.5 1.2 %copy.25 = bf16[4,256,384]{1,2,0:T(8,128)(2,1)} copy(bf16[4,256,384]{2,1,0:T(8,128)(2,1)S(1)} %bitcast.18) | data formatting | bytes 1572864 | tf_op jit(solution)/shard_map/all_to_all | solution.py:508
  62.7 15.1 %all_to_all.16 = bf16[4,256,384]{1,2,0:T(8,128)(2,1)S(1)} all-to-all(bf16[4,256,384]{1,2,0:T(8,128)(2,1)} %copy.25), channel_id=1, replica_groups=mesh['sp'=8,'tp'=4] {'tp'}, dimensions={0} | all-to-all | bytes 1572864 | tf_op jit(solution)/shard_map/all_to_all | solution.py:508
  77.9 3.5 %fusion.1 = f32[256,2048]{1,0:T(8,128)S(1)} fusion(bf16[256,1024]{0,1:T(8,128)(2,1)S(1)} %bitcast.26, bf16[1024,2048]{1,0:T(8,128)(2,1)} %param.39), kind=kOutput, calls=%fused_computation.9 | convolution fusion | flops 1073741824 | bytes 6815744 | tf_op jit(solution)/shard_map/dot_general | solution.py:515
  81.3 0.0 copy-done
  81.3 1.7 %fusion = bf16[256,2048]{1,0:T(8,128)(2,1)} fusion(f32[256,2048]{1,0:T(8,128)S(1)} %fusion.1, bf16[256,512]{0,1:T(8,128)(2,1)S(1)} %bitcast.25, bf16[512,2048]{1,0:T(8,128)(2,1)S(1)} %copy-done), kind=kOutput, calls=%fused_computation.1 | convolution fusion | flops 537919488 | bytes 5505024 | tf_op jit(solution)/shard_map/dot_general | solution.py:513
  (5 shorter events, 0.1 us)
Async XLA Ops:
  0.0 81.3 %copy-start = (bf16[512,2048]{1,0:T(8,128)(2,1)S(1)}, bf16[512,2048]{1,0:T(8,128)(2,1)}, u32[]{:S(2)}) copy-start(bf16[512,2048]{1,0:T(8,128)(2,1)} %param.38) | copy-start | bytes 6291460
  0.0 7.6 %copy-start.4 = (f32[2048]{0:T(1024)S(1)}, f32[2048]{0:T(1024)}, u32[]{:S(2)}) copy-start(f32[2048]{0:T(1024)} %param.21) | copy-start | bytes 24580
  0.0 7.6 %copy-start.1 = (bf16[1024,512]{1,0:T(8,128)(2,1)S(1)}, bf16[1024,512]{1,0:T(8,128)(2,1)}, u32[]{:S(2)}) copy-start(bf16[1024,512]{1,0:T(8,128)(2,1)} %tokens_ref.1) | copy-start | bytes 3145732
  5.3 2.3 %copy-start.2 = (bf16[2048,256]{1,0:T(8,128)(2,1)S(1)}, bf16[2048,256]{1,0:T(8,128)(2,1)}, u32[]{:S(2)}) copy-start(bf16[2048,256]{1,0:T(8,128)(2,1)} %wq_hbm.1) | copy-start | bytes 3145732
  7.7 30.6 %copy-start.3 = (f32[2,2,128,128]{3,2,1,0:T(8,128)S(1)}, f32[2,2,128,128]{3,2,1,0:T(8,128)}, u32[]{:S(2)}) copy-start(f32[2,2,128,128]{3,2,1,0:T(8,128)} %param.32) | copy-start | bytes 786436
  7.7 30.6 %copy-start.5 = (f32[2,1024]{1,0:T(2,128)S(1)}, f32[2,1024]{1,0:T(2,128)}, u32[]{:S(2)}) copy-start(f32[2,1024]{1,0:T(2,128)} %scale_ref.1) | copy-start | bytes 24580
  7.7 30.6 %copy-start.6 = (f32[2,1024]{1,0:T(2,128)S(1)}, f32[2,1024]{1,0:T(2,128)}, u32[]{:S(2)}) copy-start(f32[2,1024]{1,0:T(2,128)} %extra_ref.1) | copy-start | bytes 24580
  7.7 30.6 %copy-start.7 = (f32[2,2,128]{2,1,0:T(2,128)S(1)}, f32[2,2,128]{2,1,0:T(2,128)}, u32[]{:S(2)}) copy-start(f32[2,2,128]{2,1,0:T(2,128)} %param.33) | copy-start | bytes 6148

commit v2 on v1

v2 whole, which is shorter than its diff:
```python
import functools

import jax
import jax.numpy as jnp
from jax import lax
from jax.experimental import pallas as pl
from jax.experimental.pallas import tpu as pltpu
from jax.sharding import PartitionSpec as P

DH = 128
NEG_BIG = -1e30
LN_EPS = 1e-05
HEAD_EPS = 1e-06
RIM = 16
AUG = 144
VMEM = pltpu.VMEM
MESH = pl.DeviceIdType.MESH
F32 = jnp.float32
BF16 = jnp.bfloat16


def whole_vmem(count):
    return [pl.BlockSpec(memory_space=pltpu.VMEM)] * count


def scan_lanes(values, combine, neutral, forward_rows):
    lanes = values.shape[1]
    lane = lax.broadcasted_iota(jnp.int32, values.shape, 1)
    forward = lax.broadcasted_iota(jnp.int32, values.shape, 0) < forward_rows
    shift = 1
    while shift < lanes:
        low = jnp.where(lane >= shift, pltpu.roll(values, shift, 1), neutral)
        high = jnp.where(lane < lanes - shift, pltpu.roll(values, lanes - shift, 1), neutral)
        values = combine(values, jnp.where(forward, low, high))
        shift *= 2
    return values


def layer_kernel(
    tp_size, sp_size, heads,
    tokens_ref, gain_ref, gin_ref, gfg_ref, scale_ref, extra_ref, bias_ref,
    start_mem, start_norm, start_log, map_ref, pscale_ref, hgain_ref,
    wp_hbm, wq_hbm, wk_hbm, wv_hbm, wo_hbm, wpo_hbm, wmo_hbm,
    out_ref,
    held, normed, gate_w, wp, wq, wk, wv, wo, wpo, wmo,
    ext, q_ref, k_ref, v_ref, o_ref, gates_ref,
    adds, a_ref, acol_ref, ends_ref, locals_ref, inc_t, inc_s, exc_t, exc_s,
    send_t, send_s, recv_t, recv_s, rim_out, rims, enter_t, enter_s,
    pool_out, mem_out, lhs_pool, lhs_mem, acc,
    load_sem, far_send, far_recv, near_send, near_recv, pass_send, pass_recv,
    ts, tr, ss, sr, rs, rr, ps, pr, ms, mr,
):
    me = lax.axis_index("sp")
    group = lax.axis_index("tp")
    far = lax.rem(group + tp_size // 2, tp_size)
    near = group + 1 - 2 * lax.rem(group, 2)
    diagonal = lax.rem(near + tp_size // 2, tp_size)
    others = (far, diagonal, near)
    rows_total, width = tokens_ref.shape
    model_width = width * tp_size
    blocks = tp_size
    size = rows_total // blocks
    pairs = 2 * heads
    all_heads = gin_ref.shape[1]
    group_dim = map_ref.shape[1]
    mem_width = heads * DH
    strides = []
    stride = 1
    while stride < sp_size:
        strides.append(stride)
        stride *= 2

    barrier = pltpu.get_barrier_semaphore()
    peers = jnp.int32(len(others))
    for other in others:
        pl.semaphore_signal(barrier, inc=1, device_id={"tp": other}, device_id_type=MESH)
    for stride in strides:
        for okay, other in ((me + stride < sp_size, me + stride), (me >= stride, me - stride)):
            peers = peers + okay.astype(jnp.int32)

            @pl.when(okay)
            def _():
                pl.semaphore_signal(barrier, inc=1, device_id={"sp": other}, device_id_type=MESH)

    def load_group(pairs_of, first):
        copies = [
            pltpu.make_async_copy(source, target, load_sem.at[first + i])
            for i, (source, target) in enumerate(pairs_of)
        ]
        for copy in copies:
            copy.start()
        return copies

    loads = load_group(((wp_hbm, wp), (wq_hbm, wq), (wk_hbm, wk), (wv_hbm, wv), (wo_hbm, wo)), 0)
    gate_w[...] = jnp.concatenate(
        [ref[r].astype(F32) for ref in (gin_ref, gfg_ref) for r in range(2)], axis=0
    ).astype(BF16)
    pl.semaphore_wait(barrier, peers)

    def to_tp(source, target, send, recv, other):
        return pltpu.make_async_remote_copy(
            src_ref=source, dst_ref=target, send_sem=send, recv_sem=recv,
            device_id={"tp": other}, device_id_type=MESH,
        )

    def to_sp(source, target, send, recv, other):
        return pltpu.make_async_remote_copy(
            src_ref=source, dst_ref=target, send_sem=send, recv_sem=recv,
            device_id={"sp": other}, device_id_type=MESH,
        )

    spans = [pl.ds(c * size, size) for c in range(blocks)]
    to_far = [
        to_tp(tokens_ref.at[s], held.at[1, s], far_send.at[c], far_recv.at[c], far)
        for c, s in enumerate(spans)
    ]
    to_near = [
        to_tp(tokens_ref.at[s], held.at[0, s], near_send.at[c], near_recv.at[c], near)
        for c, s in enumerate(spans)
    ]
    onward = [
        to_tp(held.at[1, s], held.at[2, s], pass_send.at[c], pass_recv.at[c], near)
        for c, s in enumerate(spans)
    ]
    for c in range(blocks):
        to_far[c].start()
    for c in range(blocks):
        to_near[c].start()
    late_loads = load_group(((wpo_hbm, wpo), (wmo_hbm, wmo)), 5)

    bias_lane = lax.broadcasted_iota(jnp.int32, bias_ref.shape, 1)
    picked = [
        jnp.sum(jnp.where(bias_lane == group * heads + h, bias_ref[...], 0.0), axis=1, keepdims=True)
        for h in range(heads)
    ]
    bias = jnp.concatenate([picked[h][r : r + 1] for r in range(2) for h in range(heads)], axis=0)

    def own_gates(kind):
        parts = []
        for r in range(2):
            base = (2 * kind + r) * all_heads
            mine = gates_ref[base : base + heads, :]
            for other in range(1, tp_size):
                at = base + other * heads
                mine = jnp.where(group == other, gates_ref[at : at + heads, :], mine)
            parts.append(mine)
        return jnp.concatenate(parts, axis=0)

    def both_rows(ref, span):
        return jnp.concatenate(
            [jnp.broadcast_to(ref[r : r + 1, span], (heads, size)) for r in range(2)], axis=0
        )

    def project(c):
        rows = spans[c]
        views = [tokens_ref[rows, :]] + [held[slot, rows, :] for slot in range(3)]
        total = jnp.zeros((size, 1), F32)
        square = jnp.zeros((size, 1), F32)
        for view in views:
            part = view.astype(F32)
            total = total + jnp.sum(part, axis=1, keepdims=True)
            square = square + jnp.sum(part * part, axis=1, keepdims=True)
        mean = total / model_width
        inverse = lax.rsqrt(square / model_width - mean * mean + LN_EPS)
        for view, owner in zip(views, (group, near, far, diagonal)):
            columns = pl.ds(pl.multiple_of(owner * width, width), width)
            normed[:, columns] = (
                (view.astype(F32) - mean) * inverse * gain_ref[:, columns]
            ).astype(BF16)
        if c == 0:
            for load in loads:
                load.wait()
        x = normed[...]
        for weight, target in ((wk, k_ref), (wv, v_ref), (wq, q_ref), (wo, o_ref)):
            target[rows, :] = jnp.dot(x, weight[...], preferred_element_type=F32).astype(BF16)
        gates_ref[...] = lax.dot_general(
            gate_w[...], x, (((1,), (1,)), ((), ())), preferred_element_type=F32
        )
        pool = jnp.dot(x, wp[...], preferred_element_type=F32).astype(BF16)
        ext[pl.ds(RIM + c * size, size), :] = pool.astype(F32)
        if c == 0:
            rim_out[1] = pool[:RIM]
        if c == blocks - 1:
            rim_out[0] = pool[size - RIM :]

    def local_block(b):
        span = slice(b * size, (b + 1) * size)
        pre = own_gates(1) + bias
        log_sig = jnp.minimum(pre, 0.0) - jnp.log1p(jnp.exp(-jnp.abs(pre)))
        log_fg = log_sig * both_rows(scale_ref, span) + both_rows(extra_ref, span)
        falls = scan_lanes(log_fg, jnp.add, 0.0, heads)
        lifted = own_gates(0) - falls
        peaks = scan_lanes(lifted, jnp.maximum, NEG_BIG, heads)
        sources = lifted + jnp.log(F32(DH ** -0.5))
        columns = jnp.transpose(
            jnp.concatenate([peaks, jnp.zeros((128 - pairs, size), F32)], axis=0)
        )
        acol_ref[span, :] = columns
        t_at = lax.broadcasted_iota(jnp.int32, (size, size), 0)
        s_at = lax.broadcasted_iota(jnp.int32, (size, size), 1)
        for h in range(heads):
            cols = slice(h * DH, (h + 1) * DH)
            keys = k_ref[span, cols]
            vt = jnp.concatenate(
                [jnp.transpose(v_ref[span, cols].astype(F32)), jnp.ones((AUG - DH, size), F32)], axis=0
            )
            scores = lax.dot_general(
                q_ref[span, cols], keys, (((1,), (1,)), ((), ())), preferred_element_type=F32
            )
            values = jnp.concatenate([v_ref[span, cols], jnp.ones((size, DH), BF16)], axis=1)
            for r in range(2):
                p = r * heads + h
                end = size - 1 if r == 0 else 0
                top = peaks[p : p + 1, end : end + 1]
                ends_ref[b, p : p + 1, :] = jnp.broadcast_to(top, (1, 128))
                ends_ref[b, pairs + p : pairs + p + 1, :] = jnp.broadcast_to(
                    falls[p : p + 1, end : end + 1], (1, 128)
                )
                adds[p, b] = jnp.dot(
                    (vt * jnp.exp(sources[p : p + 1] - top)).astype(BF16), keys,
                    preferred_element_type=F32,
                )
                inside = (s_at <= t_at) if r == 0 else (s_at >= t_at)
                weight = jnp.exp(
                    jnp.where(inside, sources[p : p + 1] - columns[:, p : p + 1], NEG_BIG)
                )
                locals_ref[p, span, :] = jnp.dot(
                    (scores * weight).astype(BF16), values, preferred_element_type=F32
                )

    for c in range(blocks):
        to_far[c].wait_recv()
        onward[c].start()
        to_near[c].wait_recv()
        onward[c].wait_recv()
        project(c)
        local_block(c)

    def advance(p, b, state, level):
        peak = ends_ref[b, p : p + 1, :]
        fall = ends_ref[b, pairs + p : pairs + p + 1, :]
        top = jnp.maximum(level, peak)
        state = jnp.exp(level - top) * state + jnp.exp(peak - top) * adds[p, b]
        return (state, top + fall, fall)

    order = (tuple(range(blocks)), tuple(reversed(range(blocks))))
    for r in range(2):
        for h in range(heads):
            p = r * heads + h
            state = jnp.zeros((AUG, DH), F32)
            level = jnp.full((1, 128), NEG_BIG, F32)
            total_fall = jnp.zeros((1, 128), F32)
            for b in order[r]:
                state, level, fall = advance(p, b, state, level)
                total_fall = total_fall + fall
            inc_t[p] = state
            inc_s[r, h : h + 1, :] = level
            inc_s[r, heads + h : heads + h + 1, :] = total_fall
            exc_t[p] = jnp.zeros((AUG, DH), F32)
            exc_s[r, h : h + 1, :] = jnp.full((1, 128), NEG_BIG, F32)
            exc_s[r, heads + h : heads + h + 1, :] = jnp.zeros((1, 128), F32)

    def copies(level, r, other):
        return (
            to_sp(send_t.at[level, r], recv_t.at[level, r], ts.at[level, r], tr.at[level, r], other),
            to_sp(send_s.at[level, r], recv_s.at[level, r], ss.at[level, r], sr.at[level, r], other),
        )

    def route(level, r):
        stride = strides[level]
        if r == 0:
            return (me + stride < sp_size, me + stride, me >= stride)
        return (me >= stride, me - stride, me + stride < sp_size)

    def send(level):
        for r in range(2):
            okay, other, _unused = route(level, r)
            send_s[level, r] = inc_s[r]
            for h in range(heads):
                send_t[level, r, h] = inc_t[r * heads + h].astype(BF16)

            @pl.when(okay)
            def _():
                for copy in copies(level, r, other):
                    copy.start()

    def fold(level, r, t_ref, s_ref):
        for h in range(heads):
            p = r * heads + h
            early_max = recv_s[level, r, h : h + 1, :]
            early_fall = recv_s[level, r, heads + h : heads + h + 1, :]
            late_max = s_ref[r, h : h + 1, :]
            late_fall = s_ref[r, heads + h : heads + h + 1, :]
            top = jnp.maximum(early_max + late_fall, late_max)
            t_ref[p] = (
                jnp.exp(early_max + late_fall - top) * recv_t[level, r, h].astype(F32)
                + jnp.exp(late_max - top) * t_ref[p]
            )
            s_ref[r, h : h + 1, :] = top
            s_ref[r, heads + h : heads + h + 1, :] = early_fall + late_fall

    def receive(level, t_ref, s_ref, first):
        for r in range(2):
            okay, other, has = route(level, r)

            @pl.when(has)
            def _():
                if first:
                    for copy in copies(level, r, other):
                        copy.wait_recv()
                fold(level, r, t_ref, s_ref)

    def rim(side):
        other = me + 1 if side == 0 else me - 1
        return to_sp(rim_out.at[side], rims.at[side], rs.at[side], rr.at[side], other)

    rim_sends = (me + 1 < sp_size, me >= 1)
    rim_recvs = (me >= 1, me + 1 < sp_size)

    def pooling():
        for side in range(2):
            at = 0 if side == 0 else RIM + rows_total

            @pl.when(rim_recvs[side])
            def _():
                rim(side).wait_recv()
                ext[at : at + RIM, :] = rims[side].astype(F32)

            @pl.when(jnp.logical_not(rim_recvs[side]))
            def _():
                ext[at : at + RIM, :] = jnp.zeros((RIM, group_dim), F32)
        own = ext[RIM : RIM + rows_total, :]
        half = jnp.left_shift(jnp.int32(1), group)
        pooled = jnp.zeros_like(own)
        reach = RIM // 2
        for offset in range(-reach, reach):
            use = jnp.logical_and(offset >= -half, offset < half).astype(F32)
            pooled = pooled + use * ext[RIM + offset : RIM + offset + rows_total, :]
        position = me * rows_total + lax.broadcasted_iota(jnp.int32, own.shape, 0)
        count = jnp.minimum(position + half, rows_total * sp_size) - jnp.maximum(position - half, 0)
        contrast = (pooled / count.astype(F32) - own).astype(BF16)
        mapped = jnp.dot(contrast, map_ref[group], preferred_element_type=F32)
        scale = pscale_ref[:, pl.ds(pl.multiple_of(group * group_dim, group_dim), group_dim)]
        pool_out[...] = (mapped * scale).astype(BF16)

    pool_cols = pl.ds(pl.multiple_of(group * group_dim, group_dim), group_dim)
    mem_cols = pl.ds(pl.multiple_of(group * mem_width, mem_width), mem_width)

    def rows_of(owner):
        return pl.ds(pl.multiple_of(owner * size, size), size)

    pool_copies = [
        to_tp(pool_out.at[rows_of(other)], lhs_pool.at[:, pool_cols], ps.at[j], pr.at[j], other)
        for j, other in enumerate(others)
    ]
    mem_copies = [
        to_tp(mem_out.at[rows_of(other)], lhs_mem.at[:, mem_cols], ms.at[j], mr.at[j], other)
        for j, other in enumerate(others)
    ]

    def pool_product():
        lhs_pool[:, pool_cols] = pool_out[rows_of(group), :]
        for copy in pool_copies:
            copy.wait_recv()
        for load in late_loads:
            load.wait()
        acc[...] = jnp.dot(lhs_pool[...], wpo[...], preferred_element_type=F32)

    def start_pool():
        pooling()
        for copy in pool_copies:
            copy.start()

    send(0)
    for side in range(2):
        @pl.when(rim_sends[side])
        def _():
            rim(side).start()
    between = [start_pool] + [lambda: None] * len(strides)
    if len(strides) > 1:
        between[len(strides) - 1] = pool_product
    for level in range(len(strides)):
        if level > 0:
            send(level)
            receive(level - 1, exc_t, exc_s, False)
        between[level]()
        if level + 1 < len(strides):
            receive(level, inc_t, inc_s, True)
        else:
            receive(level, exc_t, exc_s, True)
    if len(strides) < 2:
        pool_product()

    for r in range(2):
        for h in range(heads):
            p = r * heads + h
            begin = start_log[r : r + 1, h : h + 1]
            late_max = exc_s[r, h : h + 1, :]
            late_fall = exc_s[r, heads + h : heads + h + 1, :]
            level = jnp.maximum(begin + late_fall, late_max)
            early = jnp.exp(begin + late_fall - level)
            late = jnp.exp(late_max - level)
            first = jnp.concatenate(
                [start_mem[r, h], jnp.broadcast_to(start_norm[r, h : h + 1, :], (AUG - DH, DH))], axis=0
            )
            state = early * first + late * exc_t[p]
            for n, b in enumerate(order[r]):
                enter_t[p, b] = jnp.concatenate(
                    [state[:DH], jnp.broadcast_to(state[DH : DH + 1], (DH, DH))], axis=0
                ).astype(BF16)
                enter_s[b, p : p + 1, :] = level
                if n + 1 < blocks:
                    state, level, _unused = advance(p, b, state, level)

    def finish(b, target, target_rows, target_cols):
        rows = rows_of(b)
        columns = acol_ref[rows, :]
        for h in range(heads):
            cols = slice(h * DH, (h + 1) * DH)
            queries = q_ref[rows, cols]
            hidden = jnp.zeros((size, DH), F32)
            for r in range(2):
                p = r * heads + h
                top = enter_s[b, p : p + 1, 0:1]
                peak = columns[:, p : p + 1]
                joint = jnp.maximum(peak, top)
                full = jnp.exp(peak - joint) * locals_ref[p, rows, :] + jnp.exp(
                    top - joint
                ) * lax.dot_general(
                    queries, enter_t[p, b], (((1,), (1,)), ((), ())), preferred_element_type=F32
                )
                hidden = hidden + full[:, :DH] / jnp.maximum(jnp.abs(full[:, DH:]), 1.0)
            centered = hidden - jnp.mean(hidden, axis=1, keepdims=True)
            variance = jnp.mean(centered * centered, axis=1, keepdims=True)
            gate = 1.0 / (1.0 + jnp.exp(-o_ref[rows, cols].astype(F32)))
            gain = hgain_ref[:, pl.ds(pl.multiple_of(group * mem_width + h * DH, DH), DH)]
            target[target_rows, target_cols(h)] = (
                centered * lax.rsqrt(variance + HEAD_EPS) * gain * gate
            ).astype(BF16)

    for other, copy in zip(others, mem_copies):
        finish(other, mem_out, rows_of(other), lambda h: slice(h * DH, (h + 1) * DH))
        copy.start()
    finish(
        group, lhs_mem, slice(None),
        lambda h: pl.ds(pl.multiple_of(group * mem_width + h * DH, DH), DH),
    )
    for copy in mem_copies:
        copy.wait_recv()
    tile = 512
    for n in range(out_ref.shape[1] // tile):
        cols = slice(n * tile, (n + 1) * tile)
        out_ref[:, cols] = (
            acc[:, cols] + jnp.dot(lhs_mem[...], wmo[:, cols], preferred_element_type=F32)
        ).astype(BF16)

    for c in range(blocks):
        to_far[c].wait_send()
        to_near[c].wait_send()
        onward[c].wait_send()
    for copy in pool_copies + mem_copies:
        copy.wait_send()
    for level in range(len(strides)):
        for r in range(2):
            okay, other, _unused = route(level, r)

            @pl.when(okay)
            def _():
                for copy in copies(level, r, other):
                    copy.wait_send()
    for side in range(2):
        @pl.when(rim_sends[side])
        def _():
            rim(side).wait_send()


def per_device(
    tokens,
    input_norm_gain,
    pooling_input_matrix,
    query_projection_matrix,
    key_projection_matrix,
    value_projection_matrix,
    output_gate_matrix,
    input_gate_matrix,
    forget_gate_matrix,
    forget_gate_bias,
    log_forget_scale,
    extra_log_forget,
    starting_memory,
    starting_normalizer,
    starting_log_scale,
    pooling_group_map,
    pooling_channel_scale,
    memory_head_gain,
    pooling_output_matrix,
    memory_output_matrix,
):
    rows, own_width = tokens.shape
    tp_size = lax.axis_size("tp")
    sp_size = lax.axis_size("sp")
    model_width = own_width * tp_size
    group_dim = pooling_input_matrix.shape[1]
    heads = query_projection_matrix.shape[1] // DH
    mem_width = heads * DH
    pairs = 2 * heads
    levels = max(1, (sp_size - 1).bit_length())
    blocks = tp_size
    size = rows // blocks
    all_heads = input_gate_matrix.shape[2]
    pool_total = pooling_output_matrix.shape[0]
    mem_total = memory_output_matrix.shape[0]
    anywhere = pl.BlockSpec(memory_space=pl.ANY)
    dma = pltpu.SemaphoreType.DMA
    return pl.pallas_call(
        functools.partial(layer_kernel, tp_size, sp_size, heads),
        out_shape=jax.ShapeDtypeStruct((size, model_width), BF16),
        in_specs=whole_vmem(13) + [anywhere] * 7,
        out_specs=pl.BlockSpec(memory_space=pltpu.VMEM),
        scratch_shapes=[
            VMEM((3, rows, own_width), BF16),
            VMEM((size, model_width), BF16),
            VMEM((4 * all_heads, model_width), BF16),
            VMEM((model_width, group_dim), BF16),
        ]
        + [VMEM((model_width, mem_width), BF16)] * 4
        + [
            VMEM((pool_total, model_width), BF16),
            VMEM((mem_total, model_width), BF16),
            VMEM((rows + 2 * RIM, group_dim), F32),
        ]
        + [VMEM((rows, mem_width), BF16)] * 4
        + [
            VMEM((4 * all_heads, size), F32),
            VMEM((pairs, blocks, AUG, DH), F32),
            VMEM((pairs, size), F32),
            VMEM((rows, 128), F32),
            VMEM((blocks, 2 * pairs, 128), F32),
            VMEM((pairs, rows, 2 * DH), F32),
            VMEM((pairs, AUG, DH), F32),
            VMEM((2, 2 * heads, 128), F32),
            VMEM((pairs, AUG, DH), F32),
            VMEM((2, 2 * heads, 128), F32),
            VMEM((levels, 2, heads, AUG, DH), BF16),
            VMEM((levels, 2, 2 * heads, 128), F32),
            VMEM((levels, 2, heads, AUG, DH), BF16),
            VMEM((levels, 2, 2 * heads, 128), F32),
            VMEM((2, RIM, group_dim), BF16),
            VMEM((2, RIM, group_dim), BF16),
            VMEM((pairs, blocks, 2 * DH, DH), BF16),
            VMEM((blocks, pairs, 128), F32),
            VMEM((rows, group_dim), BF16),
            VMEM((rows, mem_width), BF16),
            VMEM((size, pool_total), BF16),
            VMEM((size, mem_total), BF16),
            VMEM((size, model_width), F32),
        ]
        + [dma((7,))]
        + [dma((blocks,))] * 6
        + [dma((levels, 2))] * 4
        + [dma((2,))] * 2
        + [dma((3,))] * 4,
        compiler_params=pltpu.CompilerParams(
            collective_id=0, has_side_effects=True, vmem_limit_bytes=52 * 1024 * 1024
        ),
    )(
        tokens,
        input_norm_gain.reshape(1, model_width),
        input_gate_matrix.transpose(1, 2, 0),
        forget_gate_matrix.transpose(1, 2, 0),
        log_forget_scale,
        extra_log_forget,
        forget_gate_bias,
        starting_memory,
        starting_normalizer,
        starting_log_scale,
        pooling_group_map,
        pooling_channel_scale.reshape(1, pool_total),
        memory_head_gain.reshape(1, mem_total),
        pooling_input_matrix,
        query_projection_matrix,
        key_projection_matrix,
        value_projection_matrix,
        output_gate_matrix,
        pooling_output_matrix,
        memory_output_matrix,
    )


def solution(mesh):
    placed = (
        P("sp", "tp"),
        P(),
        P(None, "tp"),
        P(None, "tp"),
        P(None, "tp"),
        P(None, "tp"),
        P(None, "tp"),
        P(),
        P(),
        P(),
        P(None, "sp"),
        P(None, "sp"),
        P(None, "tp", None, None),
        P(None, "tp", None),
        P(None, "tp"),
        P(),
        P(),
        P(),
        P(),
        P(),
    )
    return jax.shard_map(
        per_device, mesh=mesh, in_specs=placed, out_specs=P(("sp", "tp"), None), check_vma=False
    )
```

time: 83.4 us -> 73.5 us (0.88); the launches traced: 83 us -> 72.1 us
  blocking collectives: 15.1 us -> 0 us
  Pallas kernels: 53.7 us -> 59.7 us
  matrix products: 5.17 us -> 0 us
  local copies, waits for them, and re-layouts: 7.46 us -> 12.4 us
  other arithmetic: 1.48 us -> 0 us
    all_to_all x1 -> x0, blocking collectives: 15.1 us -> none  [per_device(): owned = lax.all_to_all(mixed, 'tp', split_axis=0, concat_axis=1, tiled=True)]
    unnamed x16 -> x27, local copies, waits for them, and re-layouts: 0.04 us -> 12.4 us
    pallas_call x2 -> x1, Pallas kernels: 53.7 us -> 59.7 us  [per_device(): pl.pallas_call(functools.partial(layer_kernel, tp_size, sp_size, heads),...]
    dot_general x2 -> x0, matrix products: 5.17 us -> none  [the longest x1 3.46 us: per_device(): jnp.dot(mem_part, memory_output_matrix, preferred_element_type=F32)]
    dynamic_slice x3 -> x0, local copies, waits for them, and re-layouts: 2.57 us -> none  [the longest x1 1.06 us: per_device(): lax.dynamic_slice_in_dim(forget_gate_matrix, group * heads, heads, 2)]
    reshape x4 -> x0, local copies, waits for them, and re-layouts: 1.86 us -> none  [the longest x2 1.02 us: per_device(): jnp.concatenate([gate_in, gate_fg], axis=1).reshape(model_width, 2 * pairs)]
    concatenate x2 -> x0, other arithmetic: 1.48 us -> none  [the longest x1 1.43 us: per_device(): jnp.concatenate([pooling_input_matrix, gate_weight, jnp.zeros((model_widt...]
    all_to_all x1 -> x0, local copies, waits for them, and re-layouts: 1.18 us -> none  [per_device(): owned = lax.all_to_all(mixed, 'tp', split_axis=0, concat_axis=1, tiled=True)]
where the time goes in v2:
time: 73.5 us; the launch traced here: 72.1 us
  Pallas kernels  59.7 us (81%)
  local copies, waits for them, and re-layouts  12.4 us (17%)
    pallas_call x1, Pallas kernels, per_device(): pl.pallas_call(functools.partial(layer_kernel, tp_size, sp_size, heads),...  59.7 us
    unnamed x27, local copies, waits for them, and re-layouts  12.4 us

profile of v2, /device:TPU:0, one launch (start us, length us, event | category | flops | bytes accessed | tf_op | source)
XLA Modules:
  0.0 72.1 jit_solution(16163995404511734012)
XLA Ops:
  0.0 0.0 copy-start
  0.0 1.0 %copy-done = bf16[2048,128]{1,0:T(8,128)(2,1)S(1)} copy-done((bf16[2048,128]{1,0:T(8,128)(2,1)S(1)}, bf16[2048,128]{1,0:T(8,128)(2,1)}, u32[]{:S(2)}) %copy-start) | copy-done | bytes 524312
  1.0 0.0 copy-start.1
  1.0 0.9 %copy-done.1 = f32[2,2,128,128]{3,2,1,0:T(8,128)S(1)} copy-done((f32[2,2,128,128]{3,2,1,0:T(8,128)S(1)}, f32[2,2,128,128]{3,2,1,0:T(8,128)}, u32[]{:S(2)}) %copy-start.1) | copy-done | bytes 262168
  2.0 0.0 copy-start.2
  2.0 0.9 %copy-done.2 = bf16[4,128,128]{2,1,0:T(8,128)(2,1)S(1)} copy-done((bf16[4,128,128]{2,1,0:T(8,128)(2,1)S(1)}, bf16[4,128,128]{2,1,0:T(8,128)(2,1)}, u32[]{:S(2)}) %copy-start.2) | copy-done | bytes 131096
  2.9 0.0 copy-start.3
  2.9 0.8 %copy-done.3 = bf16[2048,2,8]{0,2,1:T(8,128)(2,1)S(1)} copy-done((bf16[2048,2,8]{0,2,1:T(8,128)(2,1)S(1)}, bf16[2048,2,8]{0,2,1:T(8,128)(2,1)}, u32[]{:S(2)}) %copy-start.3) | copy-done | bytes 65560
  3.7 0.0 copy-start.4
  3.7 0.8 %copy-done.4 = bf16[2048,2,8]{0,2,1:T(8,128)(2,1)S(1)} copy-done((bf16[2048,2,8]{0,2,1:T(8,128)(2,1)S(1)}, bf16[2048,2,8]{0,2,1:T(8,128)(2,1)}, u32[]{:S(2)}) %copy-start.4) | copy-done | bytes 65560
  4.6 0.0 copy-start.5
  4.6 0.7 copy-done.5
  5.3 0.0 copy-start.6
  5.3 0.7 copy-done.6
  6.0 0.0 copy-start.7
  6.0 0.7 copy-done.7
  6.7 0.0 copy-start.8
  6.7 0.7 copy-done.8
  7.4 0.0 copy-start.9
  7.4 0.7 copy-done.9
  8.0 0.0 copy-start.10
  8.0 0.7 copy-done.10
  8.7 0.0 copy-start.11
  8.7 0.7 copy-done.11
  9.4 0.0 copy-start.12
  9.4 0.7 copy-done.12
  10.1 59.7 %shard_map.190 = bf16[256,2048]{1,0:T(8,128)(2,1)} custom-call(bf16[1024,512]{1,0:T(8,128)(2,1)} %tokens_ref.1, f32[1,2048]{1,0:T(1,128)S(1)} %bitcast.7, bf16[2,8,2048]{2,1,0:T(8,128)(2,1)S(1)} %bitcast.5, bf16[2,8,2048]{2,1,0:T(8,128)(2,1)S(1)} %bitcast.6, f32[2,1024]{1,0:T(2,128)S(1)} %copy-done.6, f32[2,1024]{1,0:T(2,128)S(1)} %copy-done.7, ...), custom_call_target="tpu_custom_call" | custom-call | tf_op jit(solution)/shard_map/pallas_call | solution.py:515
  69.8 2.3 %copy.22 = bf16[256,2048]{1,0:T(8,128)(2,1)} copy(bf16[256,2048]{1,0:T(8,128)(2,1)} %shard_map.190) | data formatting | bytes 2097152
Async XLA Ops:
  0.0 1.0 %copy-start = (bf16[2048,128]{1,0:T(8,128)(2,1)S(1)}, bf16[2048,128]{1,0:T(8,128)(2,1)}, u32[]{:S(2)}) copy-start(bf16[2048,128]{1,0:T(8,128)(2,1)} %wp_hbm.1) | copy-start | bytes 1572868
  1.0 0.9 %copy-start.1 = (f32[2,2,128,128]{3,2,1,0:T(8,128)S(1)}, f32[2,2,128,128]{3,2,1,0:T(8,128)}, u32[]{:S(2)}) copy-start(f32[2,2,128,128]{3,2,1,0:T(8,128)} %start_mem.1) | copy-start | bytes 786436
  2.0 0.9 %copy-start.2 = (bf16[4,128,128]{2,1,0:T(8,128)(2,1)S(1)}, bf16[4,128,128]{2,1,0:T(8,128)(2,1)}, u32[]{:S(2)}) copy-start(bf16[4,128,128]{2,1,0:T(8,128)(2,1)} %map_ref.1) | copy-start | bytes 393220
  2.9 0.8 %copy-start.3 = (bf16[2048,2,8]{0,2,1:T(8,128)(2,1)S(1)}, bf16[2048,2,8]{0,2,1:T(8,128)(2,1)}, u32[]{:S(2)}) copy-start(bf16[2048,2,8]{0,2,1:T(8,128)(2,1)} %param.27) | copy-start | bytes 196612
  3.7 0.8 %copy-start.4 = (bf16[2048,2,8]{0,2,1:T(8,128)(2,1)S(1)}, bf16[2048,2,8]{0,2,1:T(8,128)(2,1)}, u32[]{:S(2)}) copy-start(bf16[2048,2,8]{0,2,1:T(8,128)(2,1)} %param.28) | copy-start | bytes 196612
  4.6 0.7 copy-start.5
  5.3 0.7 copy-start.6
  6.0 0.7 copy-start.7
  6.7 0.7 copy-start.8
  7.4 0.7 copy-start.9
  8.0 0.7 copy-start.10
  8.7 0.7 copy-start.11
  9.4 0.7 copy-start.12
